TPU v7x, 32 devices: a whole 2x2x4 slice. The times are simulated.
32 devices in a mesh: sp: 16 (over z, y, x), tp: 2 (over core).
Axes of the slice: x: 2, y: 2, z: 4, core: 2. Of those that a mesh axis runs over, the one named last changes fastest.
Arguments:
- tokens: bfloat16 [2048, 2048], P('sp'), may hold values from -6 to 6
- in_gain: bfloat16 [2048], replicated, may hold values from 0.099609375 to 1.8984375
- w_value: bfloat16 [2048, 4096], P('sp', 'tp'), may hold values from -0.125 to 0.125
- w_gate: bfloat16 [2048, 4096], P('sp', 'tp'), may hold values from -0.125 to 0.125
- w_in_key: bfloat16 [2048, 1024], P('sp', 'tp'), may hold values from -0.125 to 0.125
- w_read: bfloat16 [2048, 1024], P('sp', 'tp'), may hold values from -0.125 to 0.125
- w_step_fwd: bfloat16 [2048, 64], P('sp', 'tp'), may hold values from -0.25 to 0.25
- w_step_bwd: bfloat16 [2048, 64], P('sp', 'tp'), may hold values from -0.25 to 0.25
- conv_value: bfloat16 [5, 4096], P(None, 'tp'), may hold values from -2.5 to 2.5
- conv_key: bfloat16 [5, 1024], P(None, 'tp'), may hold values from -2.5 to 2.5
- conv_read: bfloat16 [5, 1024], P(None, 'tp'), may hold values from -2.5 to 2.5
- step_bias: float32 [2, 64], P(None, 'tp'), may hold values from -4 to -2
- rate: float32 [2, 64], P(None, 'tp'), may hold values from 0 to 1, as said below
- norm_gain: bfloat16 [4096], P('tp'), may hold values from 0.099609375 to 1.8984375
- w_out: bfloat16 [4096, 2048], P('tp', 'sp'), may hold values from -0.09375 to 0.09375
Outputs:
- mixed: bfloat16 [2048, 2048], P('sp')
Inputs may be any that keep to these rules, and one draw needn't show every extreme that they name: `rate`: positive decay rates, one per head and direction.
All inputs are finite; a program needn't handle non-finite values.
Results may differ from a plain program's by a relative error of at most 0.018.
Values may be sent and summed in bfloat16 or wider, within the bound.
A program may use at most 128 MiB of HBM per device.

v0:
```python
import functools
import math

import jax
import jax.numpy as jnp
from jax import lax
from jax.experimental import pallas as pl
from jax.experimental.pallas import tpu as pltpu
from jax.sharding import PartitionSpec as P

HEAD_DIM = 64
STATE = 128
KERNEL = 5
BLOCK = 128


EPSILON = 1e-05
FULL_PRECISION = lax.Precision.HIGHEST


def entering_2(x, axis, combine, identity, reverse):
    length, place = (lax.axis_size(axis), lax.axis_index(axis))
    everything = jax.tree.map(lambda part: lax.all_gather(part, axis), x)
    start = jax.tree.map(
        lambda part, zero: jnp.broadcast_to(jnp.asarray(zero, part.dtype), part.shape), x, identity
    )

    def step(k, before):
        at = length - 1 - k if reverse else k
        reached = at > place if reverse else at < place
        new = combine(before, jax.tree.map(lambda part: part[at], everything))
        return jax.tree.map(lambda a, b: jnp.where(reached, a, b), new, before)

    return lax.fori_loop(0, length, step, start)


def with_halo(cells, sides, width):
    for axis, dim in sides:
        count = lax.axis_size(axis)
        ends = count - 1
        head = lax.slice_in_dim(cells, 0, width, axis=dim)
        tail = lax.slice_in_dim(cells, cells.shape[dim] - width, cells.shape[dim], axis=dim)
        cells = jnp.concatenate(
            [
                lax.ppermute(tail, axis, [(i, (i + 1) % count) for i in range(ends)]),
                cells,
                lax.ppermute(head, axis, [((i + 1) % count, i) for i in range(ends)]),
            ],
            axis=dim,
        )
    return cells


def normalize(tensor, gain):
    return tensor * lax.rsqrt(jnp.mean(tensor * tensor, -1, keepdims=True) + EPSILON) * gain


def block_parts(values, step_size, log_decay, in_keys):
    per_group = values.shape[1] // in_keys.shape[1]
    cumulative = jnp.cumsum(log_decay, axis=0)
    log_total = cumulative[-1]
    weighting = jnp.exp(log_total[None, :] - cumulative) * step_size
    key_heads = jnp.repeat(in_keys, per_group, axis=1)
    scaled = (values.astype(jnp.float32) * weighting[:, :, None]).astype(jnp.bfloat16)
    injected = jnp.einsum("jhn,jhp->hpn", key_heads, scaled, preferred_element_type=jnp.float32)
    return (cumulative, jnp.exp(log_total), injected)


def block_step(memory, inputs):
    values, step_size, cumulative, damping, injected, in_keys, read_in = inputs
    per_group = values.shape[1] // in_keys.shape[1]
    scores = jnp.einsum("ign,jgn->ijg", read_in, in_keys, preferred_element_type=jnp.float32)
    scores = jnp.repeat(scores, per_group, axis=2)
    length = values.shape[0]
    below_mask = (jnp.arange(length)[:, None] >= jnp.arange(length)[None, :])[:, :, None]
    gaps = jnp.where(below_mask, cumulative[:, None, :] - cumulative[None, :, :], -jnp.inf)
    weights = (scores * jnp.exp(gaps) * step_size[None, :, :]).astype(jnp.bfloat16)
    within = jnp.einsum("ijh,jhp->ihp", weights, values, preferred_element_type=jnp.float32)
    read_heads = jnp.repeat(read_in.astype(jnp.float32), per_group, axis=1)
    carried = (
        jnp.einsum("ihn,hpn->ihp", read_heads, memory, precision=FULL_PRECISION)
        * jnp.exp(cumulative)[:, :, None]
    )
    memory = damping[:, None, None] * memory + injected
    return (memory, within + carried)


def blocked(tensor):
    blocks = tensor.shape[0] // BLOCK
    return tensor.reshape((blocks, BLOCK) + tensor.shape[1:])


def sweep(block_inputs, memory):
    memory, swept = lax.scan(block_step, memory, block_inputs)
    return (swept.reshape((swept.shape[0] * swept.shape[1],) + swept.shape[2:]), memory)


def settle(damping_blocks, injected_blocks, memory):

    def advance(memory, inputs):
        return (inputs[0][:, None, None] * memory + inputs[1], None)

    memory, unused = lax.scan(advance, memory, (damping_blocks, injected_blocks))
    return memory


def chain(before_pair, after_pair):
    return (
        before_pair[0] * after_pair[0],
        after_pair[0][:, None, None] * before_pair[1] + after_pair[1],
    )


def entering(damping, final_state, backward):
    identity_pair = (jnp.ones_like(damping), jnp.zeros_like(final_state))
    if backward:
        arrived = entering_2((damping, final_state), "sp", chain, identity_pair, True)
    else:
        arrived = entering_2((damping, final_state), "sp", chain, identity_pair, False)
    return arrived[1]


def body(
    tokens,
    in_gain,
    w_value,
    w_gate,
    w_in_key,
    w_read,
    w_step_fwd,
    w_step_bwd,
    conv_value,
    conv_key,
    conv_read,
    step_bias,
    rate,
    norm_gain,
    w_out,
):
    normed = normalize(tokens.astype(jnp.float32), in_gain.astype(jnp.float32)).astype(jnp.bfloat16)
    weights = (
        lax.all_gather(w_value, "sp", axis=0, tiled=True),
        lax.all_gather(w_gate, "sp", axis=0, tiled=True),
        lax.all_gather(w_in_key, "sp", axis=0, tiled=True),
        lax.all_gather(w_read, "sp", axis=0, tiled=True),
        lax.all_gather(w_step_fwd, "sp", axis=0, tiled=True),
        lax.all_gather(w_step_bwd, "sp", axis=0, tiled=True),
    )
    projected = [
        jnp.dot(normed, weight, preferred_element_type=jnp.float32).astype(jnp.bfloat16)
        for weight in weights
    ]
    value_raw, gate_raw, key_raw, read_raw, pre_fwd, pre_bwd = projected
    value_cols = value_raw.shape[1]
    key_cols = key_raw.shape[1]
    joined = jnp.concatenate([value_raw, key_raw, read_raw], axis=1)
    padded = with_halo(joined, (("sp", 0),), (KERNEL - 1) // 2)
    kernel_taps = jnp.concatenate([conv_value, conv_key, conv_read], axis=1).astype(jnp.float32)
    length = joined.shape[0]
    summed = jnp.zeros(joined.shape, jnp.float32)
    for offset in range(KERNEL):
        summed = summed + padded[offset : offset + length].astype(jnp.float32) * kernel_taps[offset]
    mixed_in = jax.nn.silu(summed).astype(jnp.bfloat16)
    head_count = value_cols // HEAD_DIM
    group_count = key_cols // STATE
    values = mixed_in[:, :value_cols].reshape(length, head_count, HEAD_DIM)
    in_keys = mixed_in[:, value_cols : value_cols + key_cols].reshape(length, group_count, STATE)
    read_in = mixed_in[:, value_cols + key_cols :].reshape(length, group_count, STATE)
    blank = jnp.zeros((head_count, HEAD_DIM, STATE), jnp.float32)
    summed_heads = jnp.zeros(values.shape, jnp.float32)
    for direction, step_pre in ((0, pre_fwd), (1, pre_bwd)):
        step_size = jax.nn.softplus(step_pre.astype(jnp.float32) + step_bias[direction])
        log_decay = -rate[direction] * step_size
        ordered = (values, step_size, log_decay, in_keys, read_in)
        if direction == 1:
            ordered = tuple((tensor[::-1] for tensor in ordered))
        value_blocks, step_blocks, decay_blocks, key_blocks, read_blocks = [
            blocked(tensor) for tensor in ordered
        ]
        cumulative_blocks, damping_blocks, injected_blocks = jax.vmap(block_parts)(
            value_blocks, step_blocks, decay_blocks, key_blocks
        )
        block_inputs = (
            value_blocks,
            step_blocks,
            cumulative_blocks,
            damping_blocks,
            injected_blocks,
            key_blocks,
            read_blocks,
        )
        damping = jnp.exp(jnp.sum(ordered[2], axis=0))
        final_state = settle(damping_blocks, injected_blocks, blank)
        arriving = entering(damping, final_state, direction == 1)
        swept, final_state = sweep(block_inputs, arriving)
        if direction == 1:
            swept = swept[::-1]
        summed_heads = summed_heads + swept
    gated_out = summed_heads * jax.nn.silu(gate_raw.astype(jnp.float32)).reshape(values.shape)
    head_gain = norm_gain.astype(jnp.float32).reshape(head_count, HEAD_DIM)
    normed_heads = normalize(gated_out, head_gain).astype(jnp.bfloat16).reshape(length, value_cols)
    out_whole = lax.all_gather(w_out, "sp", axis=1, tiled=True)
    own_rows = lax.psum_scatter(
        jnp.dot(normed_heads, out_whole, preferred_element_type=jnp.float32).astype(jnp.bfloat16),
        "tp",
        scatter_dimension=0,
        tiled=True,
    )
    return lax.all_gather(own_rows, "tp", axis=0, tiled=True)


F32 = jnp.float32
BF16 = jnp.bfloat16
LANES = 128
VMEM_SPEC = pl.BlockSpec(memory_space=pltpu.VMEM)


def greet(peers):
    barrier = pltpu.get_barrier_semaphore()
    for peer in peers:
        pl.semaphore_signal(
            barrier, inc=1, device_id=peer, device_id_type=pl.DeviceIdType.MESH
        )
    pl.semaphore_wait(barrier, len(peers))


def push(src, dst, send, recv, peer):
    copy = pltpu.make_async_remote_copy(
        src_ref=src,
        dst_ref=dst,
        send_sem=send,
        recv_sem=recv,
        device_id=peer,
        device_id_type=pl.DeviceIdType.MESH,
    )
    copy.start()
    return copy


def silu(x):
    return x * jax.nn.sigmoid(x)


def whole_kernel(
    n, q, nrm, wv, wg, wk, wr, ws, wo, taps, offsets, rates, gain, out,
    tok, wts, wst, wout, raw, gate, pre, vals, keys, reads, cums, yy, injf, injb, carf, carb, nh, full, part, both,
    tzs, tzr, tps, tpr, tss, tsr, kzs, kzr, kps, kpr, vs, vr, ss, sr, os, orr,
    as_, ar, bs, br, es, er, fs, fr, ls,
):
    s, t = lax.axis_index("sp"), lax.axis_index("tp")
    z, p = s // q, s % q
    sibling = (s, 1 - t)
    half = tok.shape[2]
    depth = wv.shape[0]
    blocks = tok.shape[0] * 2 * half // BLOCK

    def at(dz, dp):
        return lax.rem(z + dz, q) * q + lax.rem(p + dp, q)

    def span(i, size):
        return pl.ds(pl.multiple_of(i * size, size), size)

    px = p + 1 - 2 * lax.rem(p, 2)
    py = lax.rem(p + 2, q)
    pd = lax.rem(px + 2, q)
    side = {"x": (z * q + px, t), "y": (z * q + py, t)}

    def chip(dz, where):
        return lax.rem(z + q - dz, q) * q + where

    greet([(lax.rem(s + k, n), t) for k in range(1, n)] + [sibling])

    def local(src, dst, i):
        copy = pltpu.make_async_copy(src, dst, ls.at[i])
        copy.start()
        return copy

    mine = span(s, depth)
    rows = span(t, half)
    kcol, rcol = pl.ds(2 * LANES, LANES), pl.ds(3 * LANES, LANES)
    first, keyz = [], []
    for dz in range(1, q):
        first.append(push(nrm.at[rows], tok.at[s, t], tzs.at[dz], tzr.at[dz], (at(dz, 0), t)))
    for dz in range(1, q):
        grp = span(lax.rem(z + dz, q), LANES)
        keyz.append(
            [
                push(w.at[:, grp], wts.at[mine, col], kzs.at[dz, i], kzr.at[dz, i], (at(dz, 0), t))
                for i, (w, col) in enumerate(((wk, kcol), (wr, rcol)))
            ]
        )
    plane, keyp = {}, []
    for i, to in enumerate("xy"):
        plane[0, to] = push(nrm.at[rows], tok.at[s, t], tps.at[0, i], tpr.at[0, i], side[to])
    for dp in range(1, q):
        for i, (w, col) in enumerate(((wk, kcol), (wr, rcol))):
            keyp.append(
                push(
                    w.at[:, span(z, LANES)], wts.at[mine, col],
                    kps.at[i * q, dp], kpr.at[i * q, dp], (at(0, dp), t),
                )
            )
    locals_ = [
        local(nrm.at[pl.ds(0, half)], tok.at[s, 0], 0),
        local(nrm.at[pl.ds(half, half)], tok.at[s, 1], 1),
        local(wk.at[:, span(z, LANES)], wts.at[mine, kcol], 2),
        local(wr.at[:, span(z, LANES)], wts.at[mine, rcol], 3),
        local(wv.at[:, mine], wts.at[mine, pl.ds(0, LANES)], 4),
        local(wg.at[:, mine], wts.at[mine, pl.ds(LANES, LANES)], 5),
        local(ws.at[s], wst.at[pl.ds(0, ws.shape[1]), mine], 6),
    ]
    weights = []
    for k in range(1, n):
        j = lax.rem(s + k, n)
        cols = span(j, LANES)
        for i, w in enumerate((wv, wg)):
            weights.append(
                push(w.at[:, cols], wts.at[mine, pl.ds(i * LANES, LANES)], vs.at[k, i], vr.at[k, i], (j, t))
            )
        weights.append(
            push(ws.at[j], wst.at[pl.ds(0, ws.shape[1]), mine], ss.at[k], sr.at[k], (j, t))
        )
    swaps = {}

    def swap(dz, i):
        src = chip(dz, (p, px, py, pd)[i])
        swaps[dz, i] = push(tok.at[src, t], tok.at[src, t], tss.at[dz, i], tsr.at[dz, i], sibling)

    for dz in range(1, q):
        src = at(q - dz, 0)
        first[dz - 1].wait_recv()
        for i, to in enumerate("xy"):
            plane[dz, to] = push(tok.at[src, t], tok.at[src, t], tps.at[dz, i], tpr.at[dz, i], side[to])
        swap(dz, 0)
        for copy in keyz[dz - 1]:
            copy.wait_recv()
        got = wts.at[span(src, depth), pl.ds(2 * LANES, 2 * LANES)]
        for dp in range(1, q):
            keyp.append(push(got, got, kps.at[dz, dp], kpr.at[dz, dp], (at(0, dp), t)))
    outs = []
    for dz in range(1, q):
        outs.append(push(wo, wout.at[:, span(z, LANES)], os.at[dz], orr.at[dz], (at(dz, 0), t)))
    locals_.append(local(wo, wout.at[:, span(z, LANES)], 7))

    wst[ws.shape[1] :, :] = jnp.zeros((LANES - ws.shape[1], wst.shape[1]), BF16)
    seq = blocks * BLOCK
    wide = 3 * LANES
    raw[0:8, :] = jnp.zeros((8, wide), F32)
    raw[seq + 8 : seq + 16, :] = jnp.zeros((8, wide), F32)
    for copy in locals_:
        copy.wait()

    def project(plane_index):
        @pl.loop(0, q // 2)
        def _(i):
            pair = plane_index * q + 2 * i
            r0 = pl.multiple_of(pair * BLOCK, 2 * BLOCK)
            at2 = pl.ds(r0, 2 * BLOCK)
            x = tok[pl.ds(pair, 2)].reshape(2 * BLOCK, tok.shape[3])
            got = jnp.dot(x, wts[...], preferred_element_type=F32).astype(BF16)
            for i_, b_ in ((0, 0), (2, 1), (3, 2)):
                raw[pl.ds(r0 + 8, 2 * BLOCK), b_ * LANES : (b_ + 1) * LANES] = got[
                    :, i_ * LANES : (i_ + 1) * LANES
                ].astype(F32)
            gate[at2, :] = got[:, LANES : 2 * LANES]
            u = lax.dot_general(x, wst[...], (((1,), (1,)), ((), ())), preferred_element_type=F32)
            u = u.astype(BF16).astype(F32) + offsets[...]
            pre[at2, :] = jnp.maximum(u, 0.0) + jnp.log1p(jnp.exp(-jnp.abs(u)))

    quarter = half // 2

    def relay(dz):
        for i, (near_by, other) in enumerate((("x", "y"), ("y", "x"))):
            plane[dz, near_by].wait_recv()
            got = tok.at[chip(dz, (px, py)[i]), t, pl.ds(i * quarter, quarter)]
            plane[dz, other + "d"] = push(got, got, tps.at[dz, 2 + i], tpr.at[dz, 2 + i], side[other])
            swap(dz, 1 + i)

    def use(dz):
        plane[dz, "yd"].wait_recv()
        plane[dz, "xd"].wait_recv()
        swap(dz, 3)
        for i in range(q):
            if (dz, i) != (0, 0):
                swaps[dz, i].wait_recv()
        project(lax.rem(z + q - dz, q))

    for dz in range(q):
        relay(dz)
        if dz == 1:
            for copy in weights + keyp:
                copy.wait_recv()
        if dz >= 1:
            use(dz - 1)
    use(q - 1)

    @pl.loop(0, blocks, unroll=2)
    def _(i):
        r0 = pl.multiple_of(i * BLOCK, BLOCK)
        for b, dst in enumerate((vals, keys, reads)):
            window = raw[pl.ds(r0, BLOCK + 16), b * LANES : (b + 1) * LANES]
            total = jnp.zeros((BLOCK, LANES), F32)
            for k in range(KERNEL):
                lo = 8 - (KERNEL - 1) // 2 + k
                total = total + window[lo : lo + BLOCK] * taps[k : k + 1, b * LANES : (b + 1) * LANES]
            dst[pl.ds(r0, BLOCK), :] = silu(total).astype(BF16)

    ri = lax.broadcasted_iota(jnp.int32, (BLOCK, BLOCK), 0)
    ci = lax.broadcasted_iota(jnp.int32, (BLOCK, BLOCK), 1)
    low = ri >= ci
    diag = ri == ci
    fwd = ci < 2
    left = ci < HEAD_DIM
    lower = jnp.where(low, 1.0, 0.0).astype(F32)
    upper = jnp.where(ri <= ci, 1.0, 0.0).astype(F32)

    @pl.loop(0, blocks, unroll=4)
    def _(i):
        r0 = pl.multiple_of(i * BLOCK, BLOCK)
        here = pl.ds(r0, BLOCK)
        st = pre[here, :]
        ld = -rates[...] * st
        c = jnp.where(
            fwd,
            jnp.dot(lower, ld, precision=FULL_PRECISION, preferred_element_type=F32),
            jnp.dot(upper, ld, precision=FULL_PRECISION, preferred_element_type=F32),
        )
        cums[here, :] = c
        ct = c.T
        stt = st.T
        key, read, val = keys[here, :], reads[here, :], vals[here, :]
        val32 = val.astype(F32)
        score = lax.dot_general(read, key, (((1,), (1,)), ((), ())), preferred_element_type=F32)
        total = jnp.zeros((BLOCK, LANES), F32)
        for h in range(2):
            gap = jnp.where(low, c[:, h : h + 1] - ct[h : h + 1, :], c[:, h + 2 : h + 3] - ct[h + 2 : h + 3, :])
            sb = stt[h + 2 : h + 3, :]
            e = jnp.exp(gap) * jnp.where(low, stt[h : h + 1, :], sb) + jnp.where(diag, sb, 0.0)
            mask = left if h == 0 else jnp.logical_not(left)
            own = jnp.where(mask, val32, 0.0).astype(BF16)
            total = total + jnp.dot((score * e).astype(BF16), own, preferred_element_type=F32)
        yy[here, :] = total
        c_end = jnp.where(fwd[0:1], c[BLOCK - 1 : BLOCK, :], c[0:1, :])
        weighting = jnp.exp(c_end - c) * st
        key_t = key.astype(F32).T.astype(BF16)
        for d, dst in ((0, injf), (1, injb)):
            w = jnp.where(left, weighting[:, 2 * d : 2 * d + 1], weighting[:, 2 * d + 1 : 2 * d + 2])
            scaled = (val32 * w).astype(BF16)
            dst[i] = jnp.dot(key_t, scaled, preferred_element_type=F32)

    def carry(i, state, d, inj, kept):
        r0 = pl.multiple_of(i * BLOCK, BLOCK)
        here = pl.ds(r0, BLOCK)
        ec = jnp.exp(cums[here, :])
        grown = jnp.where(left, ec[:, 2 * d : 2 * d + 1], ec[:, 2 * d + 1 : 2 * d + 2])
        high = state.astype(BF16)
        rest = (state - high.astype(F32)).astype(BF16)
        read = reads[here, :]
        add = jnp.dot(read, high, preferred_element_type=F32) + jnp.dot(
            read, rest, preferred_element_type=F32
        )
        kept[here, :] = add * grown
        end = grown[BLOCK - 1 : BLOCK, :] if d == 0 else grown[0:1, :]
        return state * end + inj[i]

    def advance(i, states):
        return (
            carry(i, states[0], 0, injf, carf),
            carry(blocks - 1 - i, states[1], 1, injb, carb),
        )

    zero = jnp.zeros((STATE, LANES), F32)
    lax.fori_loop(0, blocks, advance, (zero, zero), unroll=4)

    def finish(i):
        r0 = pl.multiple_of(i * BLOCK, BLOCK)
        here = pl.ds(r0, BLOCK)
        g = (yy[here, :] + carf[here, :] + carb[here, :]) * silu(gate[here, :].astype(F32))
        sq = g * g
        m0 = jnp.sum(jnp.where(left, sq, 0.0), -1, keepdims=True) / HEAD_DIM
        m1 = jnp.sum(jnp.where(left, 0.0, sq), -1, keepdims=True) / HEAD_DIM
        scale = jnp.where(left, lax.rsqrt(m0 + EPSILON), lax.rsqrt(m1 + EPSILON))
        nh[here, :] = (g * scale * gain[...]).astype(BF16)

    away = []
    for dz in range(1, q + 1):
        to = lax.rem(z + dz, q)

        @pl.loop(0, q, unroll=4)
        def _(i):
            finish(to * q + i)

        if dz < q:
            away.append(
                push(nh.at[span(to, q * BLOCK)], full.at[:, mine], as_.at[dz], ar.at[dz], (at(dz, 0), t))
            )
    near = {}
    keep = local(nh.at[span(z, q * BLOCK)], full.at[:, mine], 8)
    for i, to in enumerate("xy"):
        near[0, to] = push(
            nh.at[span(z, q * BLOCK)], full.at[:, mine], bs.at[0, i], br.at[0, i], side[to]
        )
    for dz in range(1, q):
        away[dz - 1].wait_recv()
        got = full.at[:, span(at(q - dz, 0), LANES)]
        for i, to in enumerate("xy"):
            near[dz, to] = push(got, got, bs.at[dz, i], br.at[dz, i], side[to])
    rest_rows = q * BLOCK // 2
    for dz in range(q):
        for i, (near_by, other) in enumerate((("x", "y"), ("y", "x"))):
            near[dz, near_by].wait_recv()
            got = full.at[pl.ds(i * rest_rows, rest_rows), span(chip(dz, (px, py)[i]), LANES)]
            near[dz, other + "d"] = push(got, got, bs.at[dz, 2 + i], br.at[dz, 2 + i], side[other])
    keep.wait()
    for copy in outs + [near[dz, to] for dz in range(q) for to in ("xd", "yd")]:
        copy.wait_recv()
    legs = []
    for dp in range(1, q + 1):
        to = lax.rem(p + dp, q)
        part[to] = jnp.dot(full[span(to, BLOCK), :], wout[...], preferred_element_type=F32).astype(BF16)
    for dp in range(1, q):
        to = lax.rem(p + dp, q)
        legs.append(push(part.at[to], both.at[t, p], es.at[dp], er.at[dp], (at(0, dp), t)))
    across = [push(part.at[p], both.at[t, p], fs.at[0], fr.at[0], sibling)]
    keep = local(part.at[p], both.at[t, p], 9)
    for dp in range(1, q):
        legs[dp - 1].wait_recv()
        got = both.at[t, lax.rem(p + q - dp, q)]
        across.append(push(got, got, fs.at[dp], fr.at[dp], sibling))
    keep.wait()
    for copy in across:
        copy.wait()
    for a in range(q):
        for b in range(q):
            here = slice(a * LANES, (a + 1) * LANES)
            total = both[0, b, :, here].astype(F32) + both[1, b, :, here].astype(F32)
            out[:, (a * q + b) * LANES : (a * q + b + 1) * LANES] = total.astype(BF16)
    flat = [copy for pair in keyz for copy in pair]
    for copy in first + flat + list(plane.values()) + keyp + weights + list(swaps.values()):
        copy.wait_send()
    for copy in outs + away + list(near.values()) + legs:
        copy.wait_send()


def whole(n, q, nrm, wv, wg, wk, wr, ws, wo, taps, offsets, rates, gain):
    dma = pltpu.SemaphoreType.DMA
    vm = pltpu.VMEM
    depth = nrm.shape[0]
    width = nrm.shape[1]
    seq = n * depth
    return pl.pallas_call(
        functools.partial(whole_kernel, n, q),
        out_shape=jax.ShapeDtypeStruct((BLOCK, n * LANES), BF16),
        in_specs=[VMEM_SPEC] * 11,
        out_specs=VMEM_SPEC,
        scratch_shapes=[
            vm((n, 2, depth // 2, width), BF16),
            vm((width, 4 * LANES), BF16),
            vm((LANES, width), BF16),
            vm((wo.shape[0], q * LANES), BF16),
            vm((seq + 16, 3 * LANES), F32),
            vm((seq, LANES), BF16),
            vm((seq, LANES), F32),
            vm((seq, LANES), BF16),
            vm((seq, LANES), BF16),
            vm((seq, LANES), BF16),
            vm((seq, LANES), F32),
            vm((seq, LANES), F32),
            vm((seq // BLOCK, STATE, LANES), F32),
            vm((seq // BLOCK, STATE, LANES), F32),
            vm((seq, LANES), F32),
            vm((seq, LANES), F32),
            vm((seq, LANES), BF16),
            vm((q * BLOCK, n * LANES), BF16),
            vm((q, BLOCK, q * LANES), BF16),
            vm((2, q, BLOCK, q * LANES), BF16),
            dma((q,)), dma((q,)), dma((q, q)), dma((q, q)), dma((q, q)), dma((q, q)),
            dma((q, 2)), dma((q, 2)), dma((q + 1, q)), dma((q + 1, q)),
            dma((n, 2)), dma((n, 2)), dma((n,)), dma((n,)), dma((q,)), dma((q,)),
            dma((q,)), dma((q,)), dma((q, q)), dma((q, q)), dma((q,)), dma((q,)),
            dma((q,)), dma((q,)), dma((10,)),
        ],
        compiler_params=pltpu.CompilerParams(
            collective_id=0, has_side_effects=True, vmem_limit_bytes=56 << 20
        ),
        name="whole",
    )(nrm, wv, wg, wk, wr, ws, wo, taps, offsets, rates, gain)


def own_lanes(fwd, bwd, n):
    both = jnp.stack([fwd.reshape(fwd.shape[0], n, -1), bwd.reshape(bwd.shape[0], n, -1)], 2)
    both = both.reshape(fwd.shape[0], n, -1)
    both = jnp.pad(both, ((0, 0), (0, 0), (0, LANES - both.shape[2])))
    return both.transpose(1, 0, 2)


def headwise(
    n,
    q,
    tokens,
    in_gain,
    w_value,
    w_gate,
    w_in_key,
    w_read,
    w_step_fwd,
    w_step_bwd,
    conv_value,
    conv_key,
    conv_read,
    step_bias,
    rate,
    norm_gain,
    w_out,
):
    s = lax.axis_index("sp")
    group = s // q
    nrm = normalize(tokens.astype(F32), in_gain.astype(F32)).astype(BF16)
    steps = own_lanes(w_step_fwd, w_step_bwd, n)[:, :, :16].transpose(0, 2, 1)

    def cut(x, j):
        return lax.dynamic_slice_in_dim(x, j * LANES, LANES, 1)

    taps = jnp.concatenate([cut(conv_value, s), cut(conv_key, group), cut(conv_read, group)], 1)
    small = own_lanes(
        jnp.stack([step_bias[0], rate[0]]), jnp.stack([step_bias[1], rate[1]]), n
    )
    small = lax.dynamic_index_in_dim(small, s, 0, keepdims=False)
    gain = lax.dynamic_slice_in_dim(norm_gain, s * LANES, LANES, 0).astype(F32)[None]
    return whole(
        n, q, nrm, w_value, w_gate, w_in_key, w_read, steps, w_out,
        taps.astype(F32), small[0:1], small[1:2], gain,
    )


def whole_heads(mesh):
    n, q = mesh.shape["sp"], math.isqrt(mesh.shape["sp"])

    def run(*args):
        cols, keys = args[2].shape[1], args[4].shape[1]
        ready = (
            q * q == n
            and mesh.shape["tp"] == 2
            and cols == n * LANES
            and args[14].shape[1] == LANES
            and keys == q * LANES
            and q == 4
            and args[0].shape[1] == n * LANES
            and args[0].shape[0] == BLOCK
        )
        return headwise(n, q, *args) if ready else body(*args)

    return run


def solution(mesh):
    in_specs = (
        P("sp", None),
        P(),
        P("sp", "tp"),
        P("sp", "tp"),
        P("sp", "tp"),
        P("sp", "tp"),
        P("sp", "tp"),
        P("sp", "tp"),
        P(None, "tp"),
        P(None, "tp"),
        P(None, "tp"),
        P(None, "tp"),
        P(None, "tp"),
        P("tp"),
        P("tp", "sp"),
    )
    out_specs = P("sp", None)
    return jax.shard_map(whole_heads(mesh), mesh=mesh, in_specs=in_specs, out_specs=out_specs, check_vma=False)
```

profile of v0, /device:TPU:19, one launch (start us, length us, event | category | flops | bytes accessed | tf_op | source)
XLA Modules:
  0.0 158.7 jit_solution(13786994611912047185)
XLA Ops:
  0.0 0.0 copy-start
  0.0 1.3 bitcast_convert_fusion.gain
  1.3 0.0 copy-start.3
  1.4 1.3 fusion
  2.7 0.0 copy-done.5
  2.7 0.0 copy-done.6
  2.7 0.0 copy-done
  2.8 0.8 constant_dynamic-slice_fusion
  3.5 0.6 maximum_convert_fusion.taps
  4.1 0.0 copy-done.4
  4.1 0.1 stack_reshape.14
  4.2 0.1 copy.24
  4.3 0.1 stack_reshape.15
  4.4 0.1 copy.25
  4.5 0.2 dynamic-slice_reduce_fusion
  4.7 0.6 slice_bitcast_fusion.1
  5.2 0.0 copy-done.2
  5.2 0.0 copy-done.3
  5.3 0.1 pad_bitcast_fusion
  5.4 0.6 slice_bitcast_fusion.ws
  6.0 0.0 copy-done.1
  6.0 1.0 fusion.2.nrm
  7.0 149.8 %whole.1 = bf16[128,2048]{1,0:T(8,128)(2,1)} custom-call(bf16[128,2048]{1,0:T(8,128)(2,1)} %fusion.2.nrm, bf16[128,2048]{1,0:T(8,128)(2,1)} %wv.1, bf16[128,2048]{1,0:T(8,128)(2,1)} %wg.1, bf16[128,512]{1,0:T(8,128)(2,1)} %wk.1, bf16[128,512]{1,0:T(8,128)(2,1)} %wr.1, bf16[16,16,128]{2,1,0:T(8,128)(2,1)} %slice_bitcast_fusion.ws, bf16[2048,128]{1,0:T(8,128)(2,1)} %wo.1, ...), custom_call_target="tpu_custom_call" | custom-call | tf_op jit(solution)/shard_map/whole/pallas_call | solution.py:551
  156.9 1.9 %copy.27 = bf16[128,2048]{1,0:T(8,128)(2,1)} copy(bf16[128,2048]{1,0:T(8,128)(2,1)} %whole.1) | data formatting | bytes 1048576
  (13 shorter events, 0.1 us)
Async XLA Ops:
  0.0 2.7 %copy-start = (bf16[5,2048]{1,0:T(8,128)(2,1)S(1)}, bf16[5,2048]{1,0:T(8,128)(2,1)}, u32[]{:S(2)}) copy-start(bf16[5,2048]{1,0:T(8,128)(2,1)} %param.23) | copy-start | bytes 61444
  1.3 1.3 copy-start.5
  1.3 1.3 copy-start.6
  1.3 2.8 %copy-start.4 = (bf16[2048]{0:T(1024)(128)(2,1)S(1)}, bf16[2048]{0:T(1024)(128)(2,1)}, u32[]{:S(2)}) copy-start(bf16[2048]{0:T(1024)(128)(2,1)} %param.16) | copy-start | bytes 12292
  1.3 3.9 %copy-start.2 = (bf16[128,32]{0,1:T(8,128)(2,1)S(1)}, bf16[128,32]{0,1:T(8,128)(2,1)}, u32[]{:S(2)}) copy-start(bf16[128,32]{0,1:T(8,128)(2,1)} %param.22) | copy-start | bytes 24580
  1.3 3.9 %copy-start.3 = (bf16[128,32]{0,1:T(8,128)(2,1)S(1)}, bf16[128,32]{0,1:T(8,128)(2,1)}, u32[]{:S(2)}) copy-start(bf16[128,32]{0,1:T(8,128)(2,1)} %param.21) | copy-start | bytes 24580
  2.6 3.4 %copy-start.1 = (bf16[128,2048]{1,0:T(8,128)(2,1)S(1)}, bf16[128,2048]{1,0:T(8,128)(2,1)}, u32[]{:S(2)}) copy-start(bf16[128,2048]{1,0:T(8,128)(2,1)} %param.15) | copy-start | bytes 1572868
where the time goes:
time: 159 us
  Pallas kernels  150 us (94%)
  local copies, waits for them, and re-layouts  4.52 us (3%)
  other arithmetic  4.26 us (3%)
    pallas_call x1, Pallas kernels, whole(): pl.pallas_call(functools.partial(whole_kernel, n, q), out_shape=jax.Shape...  150 us

commit v1 on v0

--- a/solution.py
+++ b/solution.py
@@ -215,15 +215,6 @@
 VMEM_SPEC = pl.BlockSpec(memory_space=pltpu.VMEM)
 
 
-def greet(peers):
-    barrier = pltpu.get_barrier_semaphore()
-    for peer in peers:
-        pl.semaphore_signal(
-            barrier, inc=1, device_id=peer, device_id_type=pl.DeviceIdType.MESH
-        )
-    pl.semaphore_wait(barrier, len(peers))
-
-
 def push(src, dst, send, recv, peer):
     copy = pltpu.make_async_remote_copy(
         src_ref=src,
@@ -242,8 +233,9 @@
 
 
 def whole_kernel(
-    n, q, nrm, wv, wg, wk, wr, ws, wo, taps, offsets, rates, gain, out,
-    tok, wts, wst, wout, raw, gate, pre, vals, keys, reads, cums, yy, injf, injb, carf, carb, nh, full, part, both,
+    n, q, tin, ing, wv, wg, wk, wr, wsf, wsb, wo, cv, ck, cr, bias, rate, ngain, out,
+    nrm, ws, taps, gains, tok, wts, wst, wout, raw, gate, pre, vals, keys, reads, cums, yy, injf, injb, carf, carb,
+    nh, full, part, both,
     tzs, tzr, tps, tpr, tss, tsr, kzs, kzr, kps, kpr, vs, vr, ss, sr, os, orr,
     as_, ar, bs, br, es, er, fs, fr, ls,
 ):
@@ -264,11 +256,16 @@
     py = lax.rem(p + 2, q)
     pd = lax.rem(px + 2, q)
     side = {"x": (z * q + px, t), "y": (z * q + py, t)}
+    turns = (("x", "y"), ("y", "x"))
 
     def chip(dz, where):
         return lax.rem(z + q - dz, q) * q + where
 
-    greet([(lax.rem(s + k, n), t) for k in range(1, n)] + [sibling])
+    with jax.named_scope("greet"):
+        barrier = pltpu.get_barrier_semaphore()
+        peers = [(lax.rem(s + k, n), t) for k in range(1, n)] + [sibling]
+        for peer in peers:
+            pl.semaphore_signal(barrier, inc=1, device_id=peer, device_id_type=pl.DeviceIdType.MESH)
 
     def local(src, dst, i):
         copy = pltpu.make_async_copy(src, dst, ls.at[i])
@@ -278,82 +275,191 @@
     mine = span(s, depth)
     rows = span(t, half)
     kcol, rcol = pl.ds(2 * LANES, LANES), pl.ds(3 * LANES, LANES)
-    first, keyz = [], []
-    for dz in range(1, q):
-        first.append(push(nrm.at[rows], tok.at[s, t], tzs.at[dz], tzr.at[dz], (at(dz, 0), t)))
-    for dz in range(1, q):
-        grp = span(lax.rem(z + dz, q), LANES)
-        keyz.append(
-            [
-                push(w.at[:, grp], wts.at[mine, col], kzs.at[dz, i], kzr.at[dz, i], (at(dz, 0), t))
-                for i, (w, col) in enumerate(((wk, kcol), (wr, rcol)))
-            ]
+    krcol = pl.ds(2 * LANES, 2 * LANES)
+
+    with jax.named_scope("prep"):
+        locals_ = [
+            local(wk.at[:, span(z, LANES)], wts.at[mine, kcol], 2),
+            local(wr.at[:, span(z, LANES)], wts.at[mine, rcol], 3),
+            local(wv.at[:, mine], wts.at[mine, pl.ds(0, LANES)], 4),
+            local(wg.at[:, mine], wts.at[mine, pl.ds(LANES, LANES)], 5),
+        ]
+        wide_in = tin[...].astype(F32)
+        nrm[...] = normalize(wide_in, ing[...].astype(F32).reshape(1, ing.shape[0])).astype(BF16)
+        heads = wsf.shape[0]
+        slot = ws.shape[0] // n
+        row_i = lax.broadcasted_iota(jnp.int32, (n * slot, heads), 0)
+        col_i = lax.broadcasted_iota(jnp.int32, (n * slot, heads), 1)
+        place = lax.rem(row_i, slot)
+        head_of = 2 * (row_i // slot)
+        pick_f = jnp.where((place < 2) & (col_i == head_of + place), 1.0, 0.0).astype(BF16)
+        pick_b = jnp.where((place >= 2) & (col_i == head_of + place - 2), 1.0, 0.0).astype(BF16)
+        ws[...] = (
+            jnp.dot(pick_f, wsf[...], preferred_element_type=F32)
+            + jnp.dot(pick_b, wsb[...], preferred_element_type=F32)
+        ).astype(BF16)
+        own = span(s, LANES)
+        taps[0:KERNEL, 0:LANES] = cv[:, own].astype(F32)
+        taps[0:KERNEL, LANES : 2 * LANES] = ck[:, span(z, LANES)].astype(F32)
+        taps[0:KERNEL, 2 * LANES : 3 * LANES] = cr[:, span(z, LANES)].astype(F32)
+        gains[...] = ngain[...].astype(F32).reshape(n, LANES)
+        hk = lax.broadcasted_iota(jnp.int32, (heads, LANES), 0)
+        hl = lax.broadcasted_iota(jnp.int32, (heads, LANES), 1)
+        spread = jnp.where((hl < 4) & (hk == 2 * s + lax.rem(hl, 2)), 1.0, 0.0).astype(F32)
+        first_two = lax.broadcasted_iota(jnp.int32, (1, LANES), 1) < 2
+
+        def own_lanes(both_dirs):
+            got = jnp.dot(both_dirs, spread, precision=FULL_PRECISION, preferred_element_type=F32)
+            return jnp.where(first_two, got[0:1], got[1:2])
+
+        offsets = own_lanes(bias[...])
+        rates = own_lanes(rate[...])
+        wst[slot:, :] = jnp.zeros((LANES - slot, wst.shape[1]), BF16)
+        seq = blocks * BLOCK
+        wide = 3 * LANES
+        raw[0:8, :] = jnp.zeros((8, wide), F32)
+        raw[seq + 8 : seq + 16, :] = jnp.zeros((8, wide), F32)
+        for copy in locals_:
+            copy.wait()
+    with jax.named_scope("greeted"):
+        pl.semaphore_wait(barrier, len(peers))
+
+    one, last = q - 1, q
+    rising, sinking = z < q - 1, z > 0
+    unit = nrm.at[rows]
+
+    def arrival(e):
+        later = [[1, 2, 3], [0, 2, 3], [3, 1, 0], [2, 1, 0]]
+        picked = later[q - 1][e]
+        for k in range(q - 1):
+            picked = jnp.where(z == k, later[k][e], picked)
+        return picked
+
+    sources = [z] + [arrival(e) for e in range(q - 1)]
+
+    def chain(src_ref, dst_ref, sends, recvs):
+        @pl.when(rising)
+        def _():
+            push(src_ref, dst_ref, sends.at[z], recvs.at[z], (s + q, t))
+
+        @pl.when(sinking)
+        def _():
+            push(src_ref, dst_ref, sends.at[q], recvs.at[z], (s - q, t))
+
+    def remote(src, dst, send, recv, peer):
+        return pltpu.make_async_remote_copy(
+            src_ref=src, dst_ref=dst, send_sem=send, recv_sem=recv,
+            device_id=peer, device_id_type=pl.DeviceIdType.MESH,
         )
-    plane, keyp = {}, []
-    for i, to in enumerate("xy"):
-        plane[0, to] = push(nrm.at[rows], tok.at[s, t], tps.at[0, i], tpr.at[0, i], side[to])
-    for dp in range(1, q):
-        for i, (w, col) in enumerate(((wk, kcol), (wr, rcol))):
-            keyp.append(
-                push(
-                    w.at[:, span(z, LANES)], wts.at[mine, col],
-                    kps.at[i * q, dp], kpr.at[i * q, dp], (at(0, dp), t),
+
+    def onward(zs):
+        to = z + jnp.where(zs < z, 1, -1)
+        return to, (to >= 0) & (to < q)
+
+    def settle_chain(src_ref, sends, recvs, ref_of):
+        @pl.when(rising)
+        def _():
+            remote(src_ref, ref_of(z), sends.at[z], recvs.at[z], (s + q, t)).wait_send()
+
+        @pl.when(sinking)
+        def _():
+            remote(src_ref, ref_of(z), sends.at[q], recvs.at[z], (s - q, t)).wait_send()
+
+        for zs in sources[1:]:
+            to, ok = onward(zs)
+
+            @pl.when(ok)
+            def _():
+                ref = ref_of(zs)
+                remote(ref, ref, sends.at[zs], recvs.at[zs], (to * q + p, t)).wait_send()
+
+    def tok_of(zs):
+        return tok.at[zs * q + p, t]
+
+    def wout_of(zs):
+        return wout.at[:, span(zs, LANES)]
+
+    plane, keyz, keyp, weights, swaps = {}, [], {}, [], {}
+    with jax.named_scope("issue"):
+        chain(unit, tok_of(z), tzs, tzr)
+        for i, to in enumerate("xy"):
+            plane[0, to] = push(unit, tok.at[s, t], tps.at[0, i], tpr.at[0, i], side[to])
+        for dz in range(1, q):
+            grp = span(lax.rem(z + dz, q), LANES)
+            keyz.append(
+                [
+                    push(w.at[:, grp], wts.at[mine, col], kzs.at[dz, i], kzr.at[dz, i], (at(dz, 0), t))
+                    for i, (w, col) in enumerate(((wk, kcol), (wr, rcol)))
+                ]
+            )
+        got = wts.at[mine, krcol]
+        for i, to in enumerate("xy"):
+            keyp[0, to] = push(got, got, kps.at[0, i], kpr.at[0, i], side[to])
+        for k in range(1, n):
+            j = lax.rem(s + k, n)
+            cols = span(j, LANES)
+            for i, w in enumerate((wv, wg)):
+                weights.append(
+                    push(w.at[:, cols], wts.at[mine, pl.ds(i * LANES, LANES)], vs.at[k, i], vr.at[k, i], (j, t))
                 )
+            weights.append(
+                push(ws.at[span(j, slot)], wst.at[pl.ds(0, slot), mine], ss.at[k], sr.at[k], (j, t))
             )
-    locals_ = [
-        local(nrm.at[pl.ds(0, half)], tok.at[s, 0], 0),
-        local(nrm.at[pl.ds(half, half)], tok.at[s, 1], 1),
-        local(wk.at[:, span(z, LANES)], wts.at[mine, kcol], 2),
-        local(wr.at[:, span(z, LANES)], wts.at[mine, rcol], 3),
-        local(wv.at[:, mine], wts.at[mine, pl.ds(0, LANES)], 4),
-        local(wg.at[:, mine], wts.at[mine, pl.ds(LANES, LANES)], 5),
-        local(ws.at[s], wst.at[pl.ds(0, ws.shape[1]), mine], 6),
-    ]
-    weights = []
-    for k in range(1, n):
-        j = lax.rem(s + k, n)
-        cols = span(j, LANES)
-        for i, w in enumerate((wv, wg)):
-            weights.append(
-                push(w.at[:, cols], wts.at[mine, pl.ds(i * LANES, LANES)], vs.at[k, i], vr.at[k, i], (j, t))
-            )
-        weights.append(
-            push(ws.at[j], wst.at[pl.ds(0, ws.shape[1]), mine], ss.at[k], sr.at[k], (j, t))
-        )
-    swaps = {}
-
-    def swap(dz, i):
-        src = chip(dz, (p, px, py, pd)[i])
-        swaps[dz, i] = push(tok.at[src, t], tok.at[src, t], tss.at[dz, i], tsr.at[dz, i], sibling)
-
-    for dz in range(1, q):
-        src = at(q - dz, 0)
-        first[dz - 1].wait_recv()
-        for i, to in enumerate("xy"):
-            plane[dz, to] = push(tok.at[src, t], tok.at[src, t], tps.at[dz, i], tpr.at[dz, i], side[to])
-        swap(dz, 0)
-        for copy in keyz[dz - 1]:
-            copy.wait_recv()
-        got = wts.at[span(src, depth), pl.ds(2 * LANES, 2 * LANES)]
-        for dp in range(1, q):
-            keyp.append(push(got, got, kps.at[dz, dp], kpr.at[dz, dp], (at(0, dp), t)))
-    outs = []
-    for dz in range(1, q):
-        outs.append(push(wo, wout.at[:, span(z, LANES)], os.at[dz], orr.at[dz], (at(dz, 0), t)))
-    locals_.append(local(wo, wout.at[:, span(z, LANES)], 7))
-
-    wst[ws.shape[1] :, :] = jnp.zeros((LANES - ws.shape[1], wst.shape[1]), BF16)
-    seq = blocks * BLOCK
-    wide = 3 * LANES
-    raw[0:8, :] = jnp.zeros((8, wide), F32)
-    raw[seq + 8 : seq + 16, :] = jnp.zeros((8, wide), F32)
-    for copy in locals_:
-        copy.wait()
-
-    def project(plane_index):
+        locals_ = [
+            local(nrm.at[pl.ds(0, half)], tok.at[s, 0], 0),
+            local(nrm.at[pl.ds(half, half)], tok.at[s, 1], 1),
+            local(ws.at[span(s, slot)], wst.at[pl.ds(0, slot), mine], 6),
+            local(wo, wout_of(z), 7),
+        ]
+
+    def swap(e, i):
+        src = sources[e] * q + (p, px, py, pd)[i]
+        swaps[e, i] = push(tok.at[src, t], tok.at[src, t], tss.at[e, i], tsr.at[e, i], sibling)
+
+    def arrive(e):
+        with jax.named_scope("arrive"):
+            zs = sources[e]
+            ref = tok_of(zs)
+            remote(ref, ref, tzs.at[zs], tzr.at[zs], sibling).wait_recv()
+            to, ok = onward(zs)
+
+            @pl.when(ok)
+            def _():
+                push(ref, ref, tzs.at[zs], tzr.at[zs], (to * q + p, t))
+
+            for i, way in enumerate("xy"):
+                plane[e, way] = push(ref, ref, tps.at[e, i], tpr.at[e, i], side[way])
+            swap(e, 0)
+
+    quarter = half // 2
+
+    def relay(e):
+        with jax.named_scope("relay"):
+            for i, (near_by, other) in enumerate(turns):
+                plane[e, near_by].wait_recv()
+                ref = tok.at[sources[e] * q + (px, py)[i], t, pl.ds(i * quarter, quarter)]
+                plane[e, other + "d"] = push(ref, ref, tps.at[e, 2 + i], tpr.at[e, 2 + i], side[other])
+                swap(e, 1 + i)
+
+    def key_arrive(dz):
+        with jax.named_scope("key_arrive"):
+            for copy in keyz[dz - 1]:
+                copy.wait_recv()
+            ref = wts.at[span(at(q - dz, 0), depth), krcol]
+            for i, to in enumerate("xy"):
+                keyp[dz, to] = push(ref, ref, kps.at[dz, i], kpr.at[dz, i], side[to])
+
+    def key_relay(dz):
+        with jax.named_scope("key_relay"):
+            for i, (near_by, other) in enumerate(turns):
+                keyp[dz, near_by].wait_recv()
+                ref = wts.at[span(chip(dz, (px, py)[i]), depth), (kcol, rcol)[i]]
+                keyp[dz, other + "d"] = push(ref, ref, kps.at[dz, 2 + i], kpr.at[dz, 2 + i], side[other])
+
+    def project(zs):
         @pl.loop(0, q // 2)
         def _(i):
-            pair = plane_index * q + 2 * i
+            pair = zs * q + 2 * i
             r0 = pl.multiple_of(pair * BLOCK, 2 * BLOCK)
             at2 = pl.ds(r0, 2 * BLOCK)
             x = tok[pl.ds(pair, 2)].reshape(2 * BLOCK, tok.shape[3])
@@ -364,38 +470,10 @@
                 ].astype(F32)
             gate[at2, :] = got[:, LANES : 2 * LANES]
             u = lax.dot_general(x, wst[...], (((1,), (1,)), ((), ())), preferred_element_type=F32)
-            u = u.astype(BF16).astype(F32) + offsets[...]
+            u = u.astype(BF16).astype(F32) + offsets
             pre[at2, :] = jnp.maximum(u, 0.0) + jnp.log1p(jnp.exp(-jnp.abs(u)))
 
-    quarter = half // 2
-
-    def relay(dz):
-        for i, (near_by, other) in enumerate((("x", "y"), ("y", "x"))):
-            plane[dz, near_by].wait_recv()
-            got = tok.at[chip(dz, (px, py)[i]), t, pl.ds(i * quarter, quarter)]
-            plane[dz, other + "d"] = push(got, got, tps.at[dz, 2 + i], tpr.at[dz, 2 + i], side[other])
-            swap(dz, 1 + i)
-
-    def use(dz):
-        plane[dz, "yd"].wait_recv()
-        plane[dz, "xd"].wait_recv()
-        swap(dz, 3)
-        for i in range(q):
-            if (dz, i) != (0, 0):
-                swaps[dz, i].wait_recv()
-        project(lax.rem(z + q - dz, q))
-
-    for dz in range(q):
-        relay(dz)
-        if dz == 1:
-            for copy in weights + keyp:
-                copy.wait_recv()
-        if dz >= 1:
-            use(dz - 1)
-    use(q - 1)
-
-    @pl.loop(0, blocks, unroll=2)
-    def _(i):
+    def convolve(i):
         r0 = pl.multiple_of(i * BLOCK, BLOCK)
         for b, dst in enumerate((vals, keys, reads)):
             window = raw[pl.ds(r0, BLOCK + 16), b * LANES : (b + 1) * LANES]
@@ -414,12 +492,11 @@
     lower = jnp.where(low, 1.0, 0.0).astype(F32)
     upper = jnp.where(ri <= ci, 1.0, 0.0).astype(F32)
 
-    @pl.loop(0, blocks, unroll=4)
-    def _(i):
+    def within(i):
         r0 = pl.multiple_of(i * BLOCK, BLOCK)
         here = pl.ds(r0, BLOCK)
         st = pre[here, :]
-        ld = -rates[...] * st
+        ld = -rates * st
         c = jnp.where(
             fwd,
             jnp.dot(lower, ld, precision=FULL_PRECISION, preferred_element_type=F32),
@@ -437,8 +514,8 @@
             sb = stt[h + 2 : h + 3, :]
             e = jnp.exp(gap) * jnp.where(low, stt[h : h + 1, :], sb) + jnp.where(diag, sb, 0.0)
             mask = left if h == 0 else jnp.logical_not(left)
-            own = jnp.where(mask, val32, 0.0).astype(BF16)
-            total = total + jnp.dot((score * e).astype(BF16), own, preferred_element_type=F32)
+            own_val = jnp.where(mask, val32, 0.0).astype(BF16)
+            total = total + jnp.dot((score * e).astype(BF16), own_val, preferred_element_type=F32)
         yy[here, :] = total
         c_end = jnp.where(fwd[0:1], c[BLOCK - 1 : BLOCK, :], c[0:1, :])
         weighting = jnp.exp(c_end - c) * st
@@ -447,6 +524,93 @@
             w = jnp.where(left, weighting[:, 2 * d : 2 * d + 1], weighting[:, 2 * d + 1 : 2 * d + 2])
             scaled = (val32 * w).astype(BF16)
             dst[i] = jnp.dot(key_t, scaled, preferred_element_type=F32)
+
+    def use(e):
+        zs = sources[e]
+        with jax.named_scope("usewait"):
+            plane[e, "yd"].wait_recv()
+            plane[e, "xd"].wait_recv()
+            swap(e, 3)
+            for i in range(q):
+                if (e, i) != (0, 0):
+                    swaps[e, i].wait_recv()
+        with jax.named_scope("project"):
+            project(zs)
+        edge = jnp.where(zs == 0, 0, blocks - 1)
+        if e == 0:
+            start, count = zs * q + 1, q - 2
+        else:
+            start, count = zs * q + jnp.where(zs > z, -1, 1), q
+        if e == q - 1:
+            count = count + 1
+
+        def which(i):
+            return start + i if e < q - 1 else jnp.where(i < q, start + i, edge)
+
+        with jax.named_scope("conv"):
+
+            @pl.loop(0, count, unroll=count)
+            def _(i):
+                convolve(which(i))
+
+        with jax.named_scope("intra"):
+
+            @pl.loop(0, count, unroll=count)
+            def _(i):
+                within(which(i))
+
+        if e < q - 1:
+
+            @pl.when((zs == 0) | (zs == q - 1))
+            def _():
+                convolve(edge)
+                within(edge)
+
+    def wout_onward(e):
+        zs = sources[e]
+        to, ok = onward(zs)
+
+        @pl.when(ok)
+        def _():
+            ref = wout_of(zs)
+            remote(ref, ref, os.at[zs], orr.at[zs], sibling).wait_recv()
+            push(ref, ref, os.at[zs], orr.at[zs], (to * q + p, t))
+
+    def wout_arrive(e):
+        zs = sources[e]
+        to, ok = onward(zs)
+
+        @pl.when(jnp.logical_not(ok))
+        def _():
+            ref = wout_of(zs)
+            remote(ref, ref, os.at[zs], orr.at[zs], sibling).wait_recv()
+
+    arrive(1)
+    relay(0)
+    for dz in range(1, q):
+        key_arrive(dz)
+    arrive(2)
+    key_relay(0)
+    key_relay(1)
+    relay(1)
+    key_relay(2)
+    key_relay(3)
+    arrive(3)
+    chain(wo, wout_of(z), os, orr)
+    relay(2)
+    with jax.named_scope("weights"):
+        for copy in locals_:
+            copy.wait()
+        for copy in weights + [keyp[dz, to] for dz in range(q) for to in ("xd", "yd")]:
+            copy.wait_recv()
+    use(0)
+    use(1)
+    relay(3)
+    use(2)
+    with jax.named_scope("wout1"):
+        wout_onward(1)
+        wout_onward(2)
+    use(3)
 
     def carry(i, state, d, inj, kept):
         r0 = pl.multiple_of(i * BLOCK, BLOCK)
@@ -469,8 +633,11 @@
             carry(blocks - 1 - i, states[1], 1, injb, carb),
         )
 
-    zero = jnp.zeros((STATE, LANES), F32)
-    lax.fori_loop(0, blocks, advance, (zero, zero), unroll=4)
+    with jax.named_scope("carry"):
+        zero = jnp.zeros((STATE, LANES), F32)
+        lax.fori_loop(0, blocks, advance, (zero, zero), unroll=4)
+
+    gain = gains[pl.ds(s, 1), :]
 
     def finish(i):
         r0 = pl.multiple_of(i * BLOCK, BLOCK)
@@ -480,15 +647,17 @@
         m0 = jnp.sum(jnp.where(left, sq, 0.0), -1, keepdims=True) / HEAD_DIM
         m1 = jnp.sum(jnp.where(left, 0.0, sq), -1, keepdims=True) / HEAD_DIM
         scale = jnp.where(left, lax.rsqrt(m0 + EPSILON), lax.rsqrt(m1 + EPSILON))
-        nh[here, :] = (g * scale * gain[...]).astype(BF16)
+        nh[here, :] = (g * scale * gain).astype(BF16)
 
     away = []
     for dz in range(1, q + 1):
         to = lax.rem(z + dz, q)
 
-        @pl.loop(0, q, unroll=4)
-        def _(i):
-            finish(to * q + i)
+        with jax.named_scope("finish"):
+
+            @pl.loop(0, q, unroll=4)
+            def _(i):
+                finish(to * q + i)
 
         if dz < q:
             away.append(
@@ -500,60 +669,88 @@
         near[0, to] = push(
             nh.at[span(z, q * BLOCK)], full.at[:, mine], bs.at[0, i], br.at[0, i], side[to]
         )
+    with jax.named_scope("wout2"):
+        wout_onward(3)
+    rest_rows = q * BLOCK // 2
+
+    def near_relay(dz):
+        with jax.named_scope("nearwait"):
+            for i, (near_by, other) in enumerate(turns):
+                near[dz, near_by].wait_recv()
+                got = full.at[pl.ds(i * rest_rows, rest_rows), span(chip(dz, (px, py)[i]), LANES)]
+                near[dz, other + "d"] = push(got, got, bs.at[dz, 2 + i], br.at[dz, 2 + i], side[other])
+
     for dz in range(1, q):
-        away[dz - 1].wait_recv()
+        with jax.named_scope("awaywait"):
+            away[dz - 1].wait_recv()
         got = full.at[:, span(at(q - dz, 0), LANES)]
         for i, to in enumerate("xy"):
             near[dz, to] = push(got, got, bs.at[dz, i], br.at[dz, i], side[to])
-    rest_rows = q * BLOCK // 2
-    for dz in range(q):
-        for i, (near_by, other) in enumerate((("x", "y"), ("y", "x"))):
-            near[dz, near_by].wait_recv()
-            got = full.at[pl.ds(i * rest_rows, rest_rows), span(chip(dz, (px, py)[i]), LANES)]
-            near[dz, other + "d"] = push(got, got, bs.at[dz, 2 + i], br.at[dz, 2 + i], side[other])
-    keep.wait()
-    for copy in outs + [near[dz, to] for dz in range(q) for to in ("xd", "yd")]:
-        copy.wait_recv()
+        near_relay(dz - 1)
+    near_relay(q - 1)
+    with jax.named_scope("outswait"):
+        for e in range(1, q):
+            wout_arrive(e)
+    with jax.named_scope("fullwait"):
+        keep.wait()
+        for copy in [near[dz, to] for dz in range(q) for to in ("xd", "yd")]:
+            copy.wait_recv()
     legs = []
-    for dp in range(1, q + 1):
-        to = lax.rem(p + dp, q)
-        part[to] = jnp.dot(full[span(to, BLOCK), :], wout[...], preferred_element_type=F32).astype(BF16)
-    for dp in range(1, q):
+
+    def leg(dp):
         to = lax.rem(p + dp, q)
         legs.append(push(part.at[to], both.at[t, p], es.at[dp], er.at[dp], (at(0, dp), t)))
+
+    with jax.named_scope("outdot"):
+        for dp in range(1, q + 1):
+            to = lax.rem(p + dp, q)
+            part[to] = jnp.dot(full[span(to, BLOCK), :], wout[...], preferred_element_type=F32).astype(BF16)
+            if dp >= 2:
+                leg(dp - 1)
     across = [push(part.at[p], both.at[t, p], fs.at[0], fr.at[0], sibling)]
     keep = local(part.at[p], both.at[t, p], 9)
-    for dp in range(1, q):
-        legs[dp - 1].wait_recv()
-        got = both.at[t, lax.rem(p + q - dp, q)]
-        across.append(push(got, got, fs.at[dp], fr.at[dp], sibling))
-    keep.wait()
-    for copy in across:
-        copy.wait()
-    for a in range(q):
-        for b in range(q):
-            here = slice(a * LANES, (a + 1) * LANES)
-            total = both[0, b, :, here].astype(F32) + both[1, b, :, here].astype(F32)
-            out[:, (a * q + b) * LANES : (a * q + b + 1) * LANES] = total.astype(BF16)
-    flat = [copy for pair in keyz for copy in pair]
-    for copy in first + flat + list(plane.values()) + keyp + weights + list(swaps.values()):
-        copy.wait_send()
-    for copy in outs + away + list(near.values()) + legs:
-        copy.wait_send()
-
-
-def whole(n, q, nrm, wv, wg, wk, wr, ws, wo, taps, offsets, rates, gain):
+    with jax.named_scope("legswait"):
+        for dp in range(1, q):
+            legs[dp - 1].wait_recv()
+            got = both.at[t, lax.rem(p + q - dp, q)]
+            across.append(push(got, got, fs.at[dp], fr.at[dp], sibling))
+    with jax.named_scope("acrosswait"):
+        keep.wait()
+        for copy in across:
+            copy.wait()
+    with jax.named_scope("sum"):
+        for a in range(q):
+            for b in range(q):
+                here = slice(a * LANES, (a + 1) * LANES)
+                total = both[0, b, :, here].astype(F32) + both[1, b, :, here].astype(F32)
+                out[:, (a * q + b) * LANES : (a * q + b + 1) * LANES] = total.astype(BF16)
+    with jax.named_scope("sends"):
+        settle_chain(unit, tzs, tzr, tok_of)
+        settle_chain(wo, os, orr, wout_of)
+        flat = [copy for pair in keyz for copy in pair]
+        for copy in flat + list(plane.values()) + list(keyp.values()) + weights + list(swaps.values()):
+            copy.wait_send()
+        for copy in away + list(near.values()) + legs:
+            copy.wait_send()
+
+
+def whole(n, q, *args):
     dma = pltpu.SemaphoreType.DMA
     vm = pltpu.VMEM
-    depth = nrm.shape[0]
-    width = nrm.shape[1]
+    tokens, wo, wsf = args[0], args[8], args[6]
+    depth, width = tokens.shape
     seq = n * depth
+    slot = 16
     return pl.pallas_call(
         functools.partial(whole_kernel, n, q),
         out_shape=jax.ShapeDtypeStruct((BLOCK, n * LANES), BF16),
-        in_specs=[VMEM_SPEC] * 11,
+        in_specs=[VMEM_SPEC] * len(args),
         out_specs=VMEM_SPEC,
         scratch_shapes=[
+            vm((depth, width), BF16),
+            vm((n * slot, depth), BF16),
+            vm((8, 3 * LANES), F32),
+            vm((n, LANES), F32),
             vm((n, 2, depth // 2, width), BF16),
             vm((width, 4 * LANES), BF16),
             vm((LANES, width), BF16),
@@ -574,24 +771,20 @@
             vm((q * BLOCK, n * LANES), BF16),
             vm((q, BLOCK, q * LANES), BF16),
             vm((2, q, BLOCK, q * LANES), BF16),
-            dma((q,)), dma((q,)), dma((q, q)), dma((q, q)), dma((q, q)), dma((q, q)),
-            dma((q, 2)), dma((q, 2)), dma((q + 1, q)), dma((q + 1, q)),
-            dma((n, 2)), dma((n, 2)), dma((n,)), dma((n,)), dma((q,)), dma((q,)),
+            dma((q + 1,)), dma((q,)), dma((q, q)), dma((q, q)), dma((q, q)), dma((q, q)),
+            dma((q, 2)), dma((q, 2)), dma((q, q)), dma((q, q)),
+            dma((n, 2)), dma((n, 2)), dma((n,)), dma((n,)), dma((q + 1,)), dma((q,)),
             dma((q,)), dma((q,)), dma((q, q)), dma((q, q)), dma((q,)), dma((q,)),
             dma((q,)), dma((q,)), dma((10,)),
         ],
         compiler_params=pltpu.CompilerParams(
-            collective_id=0, has_side_effects=True, vmem_limit_bytes=56 << 20
+            collective_id=0, has_side_effects=True, vmem_limit_bytes=VMEM_LIMIT << 20
         ),
         name="whole",
-    )(nrm, wv, wg, wk, wr, ws, wo, taps, offsets, rates, gain)
-
-
-def own_lanes(fwd, bwd, n):
-    both = jnp.stack([fwd.reshape(fwd.shape[0], n, -1), bwd.reshape(bwd.shape[0], n, -1)], 2)
-    both = both.reshape(fwd.shape[0], n, -1)
-    both = jnp.pad(both, ((0, 0), (0, 0), (0, LANES - both.shape[2])))
-    return both.transpose(1, 0, 2)
+    )(*args)
+
+
+VMEM_LIMIT = 56
 
 
 def headwise(
@@ -613,23 +806,9 @@
     norm_gain,
     w_out,
 ):
-    s = lax.axis_index("sp")
-    group = s // q
-    nrm = normalize(tokens.astype(F32), in_gain.astype(F32)).astype(BF16)
-    steps = own_lanes(w_step_fwd, w_step_bwd, n)[:, :, :16].transpose(0, 2, 1)
-
-    def cut(x, j):
-        return lax.dynamic_slice_in_dim(x, j * LANES, LANES, 1)
-
-    taps = jnp.concatenate([cut(conv_value, s), cut(conv_key, group), cut(conv_read, group)], 1)
-    small = own_lanes(
-        jnp.stack([step_bias[0], rate[0]]), jnp.stack([step_bias[1], rate[1]]), n
-    )
-    small = lax.dynamic_index_in_dim(small, s, 0, keepdims=False)
-    gain = lax.dynamic_slice_in_dim(norm_gain, s * LANES, LANES, 0).astype(F32)[None]
     return whole(
-        n, q, nrm, w_value, w_gate, w_in_key, w_read, steps, w_out,
-        taps.astype(F32), small[0:1], small[1:2], gain,
+        n, q, tokens, in_gain, w_value, w_gate, w_in_key, w_read, w_step_fwd.T, w_step_bwd.T, w_out,
+        conv_value, conv_key, conv_read, step_bias, rate, norm_gain,
     )
 
 

time: 159 us -> 122 us (0.77)
  the two profiles are of different devices: /device:TPU:19 before, /device:TPU:0 now
where the time goes in v1:
time: 122 us
  Pallas kernels  120 us (98%)
  local copies, waits for them, and re-layouts  1.88 us (2%)
    pallas_call x1, Pallas kernels, whole(): pl.pallas_call(functools.partial(whole_kernel, n, q), out_shape=jax.Shape...  120 us

profile of v1, /device:TPU:0, one launch (start us, length us, event | category | flops | bytes accessed | tf_op | source)
XLA Modules:
  0.0 122.0 jit_solution(14146073375951622512)
XLA Ops:
  0.0 120.1 %whole.1 = bf16[128,2048]{1,0:T(8,128)(2,1)} custom-call(bf16[128,2048]{1,0:T(8,128)(2,1)} %tin.1, bf16[2048]{0:T(1024)(128)(2,1)} %ing.1, bf16[128,2048]{1,0:T(8,128)(2,1)} %wv.1, bf16[128,2048]{1,0:T(8,128)(2,1)} %wg.1, bf16[128,512]{1,0:T(8,128)(2,1)} %wk.1, bf16[128,512]{1,0:T(8,128)(2,1)} %wr.1, bf16[32,128]{1,0:T(8,128)(2,1)} %bitcast.2, ...), custom_call_target="tpu_custom_call" | custom-call | tf_op jit(solution)/shard_map/whole/pallas_call | solution.py:744
  120.1 1.9 %copy.17 = bf16[128,2048]{1,0:T(8,128)(2,1)} copy(bf16[128,2048]{1,0:T(8,128)(2,1)} %whole.1) | data formatting | bytes 1048576

commit v2 on v1

--- a/solution.py
+++ b/solution.py
@@ -233,11 +233,12 @@
 
 
 def whole_kernel(
-    n, q, tin, ing, wv, wg, wk, wr, wsf, wsb, wo, cv, ck, cr, bias, rate, ngain, out,
-    nrm, ws, taps, gains, tok, wts, wst, wout, raw, gate, pre, vals, keys, reads, cums, yy, injf, injb, carf, carb,
+    n, q, tin_h, ing_h, wv, wg, wk, wr, wsf_h, wsb_h, wo, cv_h, ck_h, cr_h, bias_h, rate_h, ngain_h, out,
+    tin, ing, wsf, wsb, cv, ck, cr, bias, rate, ngain,
+    nrm, ws, taps, gains, tok, wts, wgt, wst, wout, raw, gate, pre, sums, vals, keys, reads, cums, yy, injf, injb, carf, carb,
     nh, full, part, both,
-    tzs, tzr, tps, tpr, tss, tsr, kzs, kzr, kps, kpr, vs, vr, ss, sr, os, orr,
-    as_, ar, bs, br, es, er, fs, fr, ls,
+    tzs, tzr, tps, tpr, tss, tsr, kzs, kzr, kps, kpr, kdr, vs, vr, ss, sr, os, orr,
+    as_, ar, bs, br, bdr, es, er, fs, fr, ls, ins,
 ):
     s, t = lax.axis_index("sp"), lax.axis_index("tp")
     z, p = s // q, s % q
@@ -274,16 +275,26 @@
 
     mine = span(s, depth)
     rows = span(t, half)
-    kcol, rcol = pl.ds(2 * LANES, LANES), pl.ds(3 * LANES, LANES)
-    krcol = pl.ds(2 * LANES, 2 * LANES)
-
-    with jax.named_scope("prep"):
+    kcol, rcol = pl.ds(LANES, LANES), pl.ds(2 * LANES, LANES)
+    krcol = pl.ds(LANES, 2 * LANES)
+
+    with jax.named_scope("load"):
+        held = (
+            (tin_h, tin), (ing_h, ing), (wsf_h, wsf), (wsb_h, wsb), (cv_h, cv), (ck_h, ck), (cr_h, cr),
+            (bias_h, bias), (rate_h, rate), (ngain_h, ngain),
+        )
+        loads = [pltpu.make_async_copy(src, dst, ins.at[i]) for i, (src, dst) in enumerate(held)]
+        for copy in loads:
+            copy.start()
         locals_ = [
             local(wk.at[:, span(z, LANES)], wts.at[mine, kcol], 2),
             local(wr.at[:, span(z, LANES)], wts.at[mine, rcol], 3),
             local(wv.at[:, mine], wts.at[mine, pl.ds(0, LANES)], 4),
-            local(wg.at[:, mine], wts.at[mine, pl.ds(LANES, LANES)], 5),
+            local(wg.at[:, mine], wgt.at[mine], 5),
         ]
+        for copy in loads:
+            copy.wait()
+    with jax.named_scope("prep"):
         wide_in = tin[...].astype(F32)
         nrm[...] = normalize(wide_in, ing[...].astype(F32).reshape(1, ing.shape[0])).astype(BF16)
         heads = wsf.shape[0]
@@ -303,17 +314,20 @@
         taps[0:KERNEL, LANES : 2 * LANES] = ck[:, span(z, LANES)].astype(F32)
         taps[0:KERNEL, 2 * LANES : 3 * LANES] = cr[:, span(z, LANES)].astype(F32)
         gains[...] = ngain[...].astype(F32).reshape(n, LANES)
-        hk = lax.broadcasted_iota(jnp.int32, (heads, LANES), 0)
-        hl = lax.broadcasted_iota(jnp.int32, (heads, LANES), 1)
-        spread = jnp.where((hl < 4) & (hk == 2 * s + lax.rem(hl, 2)), 1.0, 0.0).astype(F32)
-        first_two = lax.broadcasted_iota(jnp.int32, (1, LANES), 1) < 2
-
-        def own_lanes(both_dirs):
-            got = jnp.dot(both_dirs, spread, precision=FULL_PRECISION, preferred_element_type=F32)
-            return jnp.where(first_two, got[0:1], got[1:2])
-
-        offsets = own_lanes(bias[...])
-        rates = own_lanes(rate[...])
+        lanes_of = lax.broadcasted_iota(jnp.int32, (8, heads), 1)
+        rows_of = lax.broadcasted_iota(jnp.int32, (8, heads), 0)
+        spread = jnp.where((rows_of < 4) & (lanes_of == 2 * s + lax.rem(rows_of, 2)), 1.0, 0.0).astype(F32)
+        first_two = lax.broadcasted_iota(jnp.int32, (8, 1), 0) < 2
+        across_lanes = (((1,), (1,)), ((), ()))
+
+        def own_rows(both_dirs):
+            got = lax.dot_general(
+                spread, both_dirs, across_lanes, precision=FULL_PRECISION, preferred_element_type=F32
+            )
+            return jnp.where(first_two, got[:, 0:1], got[:, 1:2])
+
+        offsets = own_rows(bias[...])
+        rates = own_rows(rate[...])
         wst[slot:, :] = jnp.zeros((LANES - slot, wst.shape[1]), BF16)
         seq = blocks * BLOCK
         wide = 3 * LANES
@@ -352,6 +366,12 @@
             device_id=peer, device_id_type=pl.DeviceIdType.MESH,
         )
 
+    def landed(ref, sem):
+        remote(ref, ref, sem, sem, sibling).wait_recv()
+
+    def left_here(ref, sem):
+        remote(ref, ref, sem, sem, sibling).wait_send()
+
     def onward(zs):
         to = z + jnp.where(zs < z, 1, -1)
         return to, (to >= 0) & (to < q)
@@ -383,27 +403,25 @@
     with jax.named_scope("issue"):
         chain(unit, tok_of(z), tzs, tzr)
         for i, to in enumerate("xy"):
-            plane[0, to] = push(unit, tok.at[s, t], tps.at[0, i], tpr.at[0, i], side[to])
+            plane[0, to] = push(unit, tok.at[s, t], tps.at[0], tpr.at[0, i], side[to])
         for dz in range(1, q):
             grp = span(lax.rem(z + dz, q), LANES)
             keyz.append(
                 [
-                    push(w.at[:, grp], wts.at[mine, col], kzs.at[dz, i], kzr.at[dz, i], (at(dz, 0), t))
+                    push(w.at[:, grp], wts.at[mine, col], kzs.at[0], kzr.at[dz], (at(dz, 0), t))
                     for i, (w, col) in enumerate(((wk, kcol), (wr, rcol)))
                 ]
             )
         got = wts.at[mine, krcol]
         for i, to in enumerate("xy"):
-            keyp[0, to] = push(got, got, kps.at[0, i], kpr.at[0, i], side[to])
+            keyp[0, to] = push(got, got, kps.at[0], kpr.at[0, i], side[to])
         for k in range(1, n):
             j = lax.rem(s + k, n)
-            cols = span(j, LANES)
-            for i, w in enumerate((wv, wg)):
-                weights.append(
-                    push(w.at[:, cols], wts.at[mine, pl.ds(i * LANES, LANES)], vs.at[k, i], vr.at[k, i], (j, t))
-                )
             weights.append(
-                push(ws.at[span(j, slot)], wst.at[pl.ds(0, slot), mine], ss.at[k], sr.at[k], (j, t))
+                push(wv.at[:, span(j, LANES)], wts.at[mine, pl.ds(0, LANES)], vs.at[0], vr.at[0], (j, t))
+            )
+            weights.append(
+                push(ws.at[span(j, slot)], wst.at[pl.ds(0, slot), mine], ss.at[0], sr.at[0], (j, t))
             )
         locals_ = [
             local(nrm.at[pl.ds(0, half)], tok.at[s, 0], 0),
@@ -412,9 +430,16 @@
             local(wo, wout_of(z), 7),
         ]
 
+    gates = []
+
+    def send_gates():
+        for k in range(1, n):
+            j = lax.rem(s + k, n)
+            gates.append(push(wg.at[:, span(j, LANES)], wgt.at[mine], vs.at[1], vr.at[1], (j, t)))
+
     def swap(e, i):
         src = sources[e] * q + (p, px, py, pd)[i]
-        swaps[e, i] = push(tok.at[src, t], tok.at[src, t], tss.at[e, i], tsr.at[e, i], sibling)
+        swaps[e, i] = push(tok.at[src, t], tok.at[src, t], tss.at[0], tsr.at[e], sibling)
 
     def arrive(e):
         with jax.named_scope("arrive"):
@@ -427,9 +452,11 @@
             def _():
                 push(ref, ref, tzs.at[zs], tzr.at[zs], (to * q + p, t))
 
-            for i, way in enumerate("xy"):
-                plane[e, way] = push(ref, ref, tps.at[e, i], tpr.at[e, i], side[way])
-            swap(e, 0)
+    def spread_plane(e):
+        ref = tok_of(sources[e])
+        for i, way in enumerate("xy"):
+            plane[e, way] = push(ref, ref, tps.at[0], tpr.at[e, i], side[way])
+        swap(e, 0)
 
     quarter = half // 2
 
@@ -438,40 +465,67 @@
             for i, (near_by, other) in enumerate(turns):
                 plane[e, near_by].wait_recv()
                 ref = tok.at[sources[e] * q + (px, py)[i], t, pl.ds(i * quarter, quarter)]
-                plane[e, other + "d"] = push(ref, ref, tps.at[e, 2 + i], tpr.at[e, 2 + i], side[other])
+                plane[e, other + "d"] = push(ref, ref, tps.at[0], tpr.at[e, 2], side[other])
                 swap(e, 1 + i)
 
     def key_arrive(dz):
         with jax.named_scope("key_arrive"):
-            for copy in keyz[dz - 1]:
-                copy.wait_recv()
+            landed(wgt.at[pl.ds(0, 2 * depth)], kzr.at[dz])
             ref = wts.at[span(at(q - dz, 0), depth), krcol]
             for i, to in enumerate("xy"):
-                keyp[dz, to] = push(ref, ref, kps.at[dz, i], kpr.at[dz, i], side[to])
+                keyp[dz, to] = push(ref, ref, kps.at[0], kpr.at[dz, i], side[to])
 
     def key_relay(dz):
         with jax.named_scope("key_relay"):
             for i, (near_by, other) in enumerate(turns):
                 keyp[dz, near_by].wait_recv()
                 ref = wts.at[span(chip(dz, (px, py)[i]), depth), (kcol, rcol)[i]]
-                keyp[dz, other + "d"] = push(ref, ref, kps.at[dz, 2 + i], kpr.at[dz, 2 + i], side[other])
+                keyp[dz, other + "d"] = push(ref, ref, kps.at[0], kdr.at[0], side[other])
+
+    ri = lax.broadcasted_iota(jnp.int32, (BLOCK, BLOCK), 0)
+    ci = lax.broadcasted_iota(jnp.int32, (BLOCK, BLOCK), 1)
+    low = ri >= ci
+    diag = ri == ci
+    left = ci < HEAD_DIM
+    until = jnp.where(ri <= ci, 1.0, 0.0).astype(BF16)
+    since = jnp.where(low, 1.0, 0.0).astype(BF16)
+    sums_of = jnp.concatenate([until, since], axis=1)
+    pick = jnp.where(ri[0:8] == ci[0:8], 1.0, 0.0).astype(BF16)
 
     def project(zs):
-        @pl.loop(0, q // 2)
-        def _(i):
-            pair = zs * q + 2 * i
-            r0 = pl.multiple_of(pair * BLOCK, 2 * BLOCK)
-            at2 = pl.ds(r0, 2 * BLOCK)
-            x = tok[pl.ds(pair, 2)].reshape(2 * BLOCK, tok.shape[3])
-            got = jnp.dot(x, wts[...], preferred_element_type=F32).astype(BF16)
-            for i_, b_ in ((0, 0), (2, 1), (3, 2)):
-                raw[pl.ds(r0 + 8, 2 * BLOCK), b_ * LANES : (b_ + 1) * LANES] = got[
-                    :, i_ * LANES : (i_ + 1) * LANES
-                ].astype(F32)
-            gate[at2, :] = got[:, LANES : 2 * LANES]
-            u = lax.dot_general(x, wst[...], (((1,), (1,)), ((), ())), preferred_element_type=F32)
-            u = u.astype(BF16).astype(F32) + offsets
-            pre[at2, :] = jnp.maximum(u, 0.0) + jnp.log1p(jnp.exp(-jnp.abs(u)))
+        r0 = pl.multiple_of(zs * q * BLOCK, q * BLOCK)
+        whole_plane = pl.ds(r0, q * BLOCK)
+        x = tok[pl.ds(zs * q, q)].reshape(q * BLOCK, tok.shape[3])
+        got = jnp.dot(x, wts[...], preferred_element_type=F32).astype(BF16)
+        raw[pl.ds(r0 + 8, q * BLOCK), :] = got[:, 0 : 3 * LANES].astype(F32)
+        u = lax.dot_general(pick, got[:, 3 * LANES :], across_lanes, preferred_element_type=F32) + offsets
+        steps = jnp.maximum(u, 0.0) + jnp.log1p(jnp.exp(-jnp.abs(u)))
+        pre[:, whole_plane] = steps
+        decay = -rates * steps
+        parts = []
+        for b in range(q):
+            rest = decay[:, b * BLOCK : (b + 1) * BLOCK]
+            for _ in range(3):
+                piece = rest.astype(BF16).astype(F32)
+                parts.append(piece)
+                rest = rest - piece
+        summed = jnp.dot(jnp.concatenate(parts, axis=0).astype(BF16), sums_of, preferred_element_type=F32)
+        for b in range(q):
+            at_b = pl.ds(pl.multiple_of((zs * q + b) * BLOCK, BLOCK), BLOCK)
+            got = [summed[24 * b + 8 * k : 24 * b + 8 * k + 8] for k in range(3)]
+            both_sums = got[0] + (got[1] + got[2])
+            c = jnp.where(first_two, both_sums[:, 0:BLOCK], both_sums[:, BLOCK:])
+            c_end = jnp.where(first_two, c[:, BLOCK - 1 : BLOCK], c[:, 0:1])
+            sums[:, at_b] = c
+            weighting = jnp.exp(c_end - c) * steps[:, b * BLOCK : (b + 1) * BLOCK]
+            stacked = jnp.concatenate([c, weighting, jnp.exp(c), jnp.zeros((LANES - 24, BLOCK), F32)], axis=0)
+            cums[at_b, :] = stacked.T
+
+    def open_gate(zs):
+        with jax.named_scope("gate"):
+            x = tok[pl.ds(zs * q, q)].reshape(q * BLOCK, tok.shape[3])
+            here = pl.ds(pl.multiple_of(zs * q * BLOCK, q * BLOCK), q * BLOCK)
+            gate[here, :] = jnp.dot(x, wgt[...], preferred_element_type=F32).astype(BF16)
 
     def convolve(i):
         r0 = pl.multiple_of(i * BLOCK, BLOCK)
@@ -483,31 +537,13 @@
                 total = total + window[lo : lo + BLOCK] * taps[k : k + 1, b * LANES : (b + 1) * LANES]
             dst[pl.ds(r0, BLOCK), :] = silu(total).astype(BF16)
 
-    ri = lax.broadcasted_iota(jnp.int32, (BLOCK, BLOCK), 0)
-    ci = lax.broadcasted_iota(jnp.int32, (BLOCK, BLOCK), 1)
-    low = ri >= ci
-    diag = ri == ci
-    fwd = ci < 2
-    left = ci < HEAD_DIM
-    lower = jnp.where(low, 1.0, 0.0).astype(F32)
-    upper = jnp.where(ri <= ci, 1.0, 0.0).astype(F32)
-
     def within(i):
         r0 = pl.multiple_of(i * BLOCK, BLOCK)
         here = pl.ds(r0, BLOCK)
-        st = pre[here, :]
-        ld = -rates * st
-        c = jnp.where(
-            fwd,
-            jnp.dot(lower, ld, precision=FULL_PRECISION, preferred_element_type=F32),
-            jnp.dot(upper, ld, precision=FULL_PRECISION, preferred_element_type=F32),
-        )
-        cums[here, :] = c
-        ct = c.T
-        stt = st.T
+        c, ct, stt = cums[here, :], sums[:, here], pre[:, here]
         key, read, val = keys[here, :], reads[here, :], vals[here, :]
         val32 = val.astype(F32)
-        score = lax.dot_general(read, key, (((1,), (1,)), ((), ())), preferred_element_type=F32)
+        score = lax.dot_general(read, key, across_lanes, preferred_element_type=F32)
         total = jnp.zeros((BLOCK, LANES), F32)
         for h in range(2):
             gap = jnp.where(low, c[:, h : h + 1] - ct[h : h + 1, :], c[:, h + 2 : h + 3] - ct[h + 2 : h + 3, :])
@@ -517,23 +553,18 @@
             own_val = jnp.where(mask, val32, 0.0).astype(BF16)
             total = total + jnp.dot((score * e).astype(BF16), own_val, preferred_element_type=F32)
         yy[here, :] = total
-        c_end = jnp.where(fwd[0:1], c[BLOCK - 1 : BLOCK, :], c[0:1, :])
-        weighting = jnp.exp(c_end - c) * st
         key_t = key.astype(F32).T.astype(BF16)
         for d, dst in ((0, injf), (1, injb)):
-            w = jnp.where(left, weighting[:, 2 * d : 2 * d + 1], weighting[:, 2 * d + 1 : 2 * d + 2])
+            w = jnp.where(left, c[:, 8 + 2 * d : 9 + 2 * d], c[:, 9 + 2 * d : 10 + 2 * d])
             scaled = (val32 * w).astype(BF16)
             dst[i] = jnp.dot(key_t, scaled, preferred_element_type=F32)
 
     def use(e):
         zs = sources[e]
         with jax.named_scope("usewait"):
-            plane[e, "yd"].wait_recv()
-            plane[e, "xd"].wait_recv()
+            landed(tok.at[0, 0], tpr.at[e, 2])
             swap(e, 3)
-            for i in range(q):
-                if (e, i) != (0, 0):
-                    swaps[e, i].wait_recv()
+            landed(tok.at[pl.ds(0, q if e else q - 1), 0], tsr.at[e])
         with jax.named_scope("project"):
             project(zs)
         edge = jnp.where(zs == 0, 0, blocks - 1)
@@ -547,6 +578,8 @@
         def which(i):
             return start + i if e < q - 1 else jnp.where(i < q, start + i, edge)
 
+        if e == q - 1:
+            open_gate(zs)
         with jax.named_scope("conv"):
 
             @pl.loop(0, count, unroll=count)
@@ -589,24 +622,36 @@
     relay(0)
     for dz in range(1, q):
         key_arrive(dz)
+    key_relay(0)
+    spread_plane(1)
+    for dz in range(1, q):
+        key_relay(dz)
     arrive(2)
-    key_relay(0)
-    key_relay(1)
+    spread_plane(2)
     relay(1)
-    key_relay(2)
-    key_relay(3)
-    arrive(3)
-    chain(wo, wout_of(z), os, orr)
-    relay(2)
+    send_gates()
     with jax.named_scope("weights"):
         for copy in locals_:
             copy.wait()
-        for copy in weights + [keyp[dz, to] for dz in range(q) for to in ("xd", "yd")]:
-            copy.wait_recv()
+        landed(wgt.at[pl.ds(0, (n - 1) * depth)], vr.at[0])
+        landed(ws.at[pl.ds(0, (n - 1) * slot)], sr.at[0])
+        landed(wgt.at[pl.ds(0, 2 * q * depth)], kdr.at[0])
+    with jax.named_scope("turn"):
+        for k in range(wst.shape[1] // LANES):
+            chunk = slice(k * LANES, (k + 1) * LANES)
+            wts[chunk, 3 * LANES :] = wst[:, chunk].astype(F32).T.astype(BF16)
     use(0)
+    arrive(3)
+    spread_plane(3)
+    chain(wo, wout_of(z), os, orr)
+    relay(2)
     use(1)
     relay(3)
     use(2)
+    with jax.named_scope("gates"):
+        landed(wgt.at[pl.ds(0, (n - 1) * depth)], vr.at[1])
+    for e in range(q - 1):
+        open_gate(sources[e])
     with jax.named_scope("wout1"):
         wout_onward(1)
         wout_onward(2)
@@ -615,8 +660,7 @@
     def carry(i, state, d, inj, kept):
         r0 = pl.multiple_of(i * BLOCK, BLOCK)
         here = pl.ds(r0, BLOCK)
-        ec = jnp.exp(cums[here, :])
-        grown = jnp.where(left, ec[:, 2 * d : 2 * d + 1], ec[:, 2 * d + 1 : 2 * d + 2])
+        grown = jnp.where(left, cums[here, 16 + 2 * d : 17 + 2 * d], cums[here, 17 + 2 * d : 18 + 2 * d])
         high = state.astype(BF16)
         rest = (state - high.astype(F32)).astype(BF16)
         read = reads[here, :]
@@ -661,16 +705,14 @@
 
         if dz < q:
             away.append(
-                push(nh.at[span(to, q * BLOCK)], full.at[:, mine], as_.at[dz], ar.at[dz], (at(dz, 0), t))
+                push(nh.at[span(to, q * BLOCK)], full.at[:, mine], as_.at[0], ar.at[dz], (at(dz, 0), t))
             )
     near = {}
     keep = local(nh.at[span(z, q * BLOCK)], full.at[:, mine], 8)
     for i, to in enumerate("xy"):
         near[0, to] = push(
-            nh.at[span(z, q * BLOCK)], full.at[:, mine], bs.at[0, i], br.at[0, i], side[to]
+            nh.at[span(z, q * BLOCK)], full.at[:, mine], bs.at[0], br.at[0, i], side[to]
         )
-    with jax.named_scope("wout2"):
-        wout_onward(3)
     rest_rows = q * BLOCK // 2
 
     def near_relay(dz):
@@ -678,28 +720,30 @@
             for i, (near_by, other) in enumerate(turns):
                 near[dz, near_by].wait_recv()
                 got = full.at[pl.ds(i * rest_rows, rest_rows), span(chip(dz, (px, py)[i]), LANES)]
-                near[dz, other + "d"] = push(got, got, bs.at[dz, 2 + i], br.at[dz, 2 + i], side[other])
+                near[dz, other + "d"] = push(got, got, bs.at[0], bdr.at[0], side[other])
 
     for dz in range(1, q):
         with jax.named_scope("awaywait"):
             away[dz - 1].wait_recv()
         got = full.at[:, span(at(q - dz, 0), LANES)]
         for i, to in enumerate("xy"):
-            near[dz, to] = push(got, got, bs.at[dz, i], br.at[dz, i], side[to])
+            near[dz, to] = push(got, got, bs.at[0], br.at[dz, i], side[to])
         near_relay(dz - 1)
+        if dz == 2:
+            with jax.named_scope("wout2"):
+                wout_onward(3)
     near_relay(q - 1)
     with jax.named_scope("outswait"):
         for e in range(1, q):
             wout_arrive(e)
     with jax.named_scope("fullwait"):
         keep.wait()
-        for copy in [near[dz, to] for dz in range(q) for to in ("xd", "yd")]:
-            copy.wait_recv()
+        landed(full.at[pl.ds(0, BLOCK)], bdr.at[0])
     legs = []
 
     def leg(dp):
         to = lax.rem(p + dp, q)
-        legs.append(push(part.at[to], both.at[t, p], es.at[dp], er.at[dp], (at(0, dp), t)))
+        legs.append(push(part.at[to], both.at[t, p], es.at[0], er.at[dp], (at(0, dp), t)))
 
     with jax.named_scope("outdot"):
         for dp in range(1, q + 1):
@@ -713,11 +757,10 @@
         for dp in range(1, q):
             legs[dp - 1].wait_recv()
             got = both.at[t, lax.rem(p + q - dp, q)]
-            across.append(push(got, got, fs.at[dp], fr.at[dp], sibling))
+            across.append(push(got, got, fs.at[0], fr.at[0], sibling))
     with jax.named_scope("acrosswait"):
         keep.wait()
-        for copy in across:
-            copy.wait()
+        landed(part, fr.at[0])
     with jax.named_scope("sum"):
         for a in range(q):
             for b in range(q):
@@ -727,11 +770,17 @@
     with jax.named_scope("sends"):
         settle_chain(unit, tzs, tzr, tok_of)
         settle_chain(wo, os, orr, wout_of)
-        flat = [copy for pair in keyz for copy in pair]
-        for copy in flat + list(plane.values()) + list(keyp.values()) + weights + list(swaps.values()):
-            copy.wait_send()
-        for copy in away + list(near.values()) + legs:
-            copy.wait_send()
+        left_here(tok.at[pl.ds(0, 3 * q), 0], tps.at[0])
+        left_here(tok.at[pl.ds(0, n - 1), 0], tss.at[0])
+        left_here(wgt.at[pl.ds(0, 2 * (q - 1) * depth)], kzs.at[0])
+        left_here(wts.at[pl.ds(0, 6 * depth)], kps.at[0])
+        left_here(wgt.at[pl.ds(0, (n - 1) * depth)], vs.at[0])
+        left_here(wgt.at[pl.ds(0, (n - 1) * depth)], vs.at[1])
+        left_here(ws.at[pl.ds(0, (n - 1) * slot)], ss.at[0])
+        left_here(nh.at[pl.ds(0, (q - 1) * q * BLOCK)], as_.at[0])
+        left_here(full.at[pl.ds(0, 3 * BLOCK)], bs.at[0])
+        left_here(part.at[pl.ds(0, q - 1)], es.at[0])
+        left_here(part, fs.at[0])
 
 
 def whole(n, q, *args):
@@ -744,20 +793,23 @@
     return pl.pallas_call(
         functools.partial(whole_kernel, n, q),
         out_shape=jax.ShapeDtypeStruct((BLOCK, n * LANES), BF16),
-        in_specs=[VMEM_SPEC] * len(args),
+        in_specs=[HBM_SPEC] * len(args),
         out_specs=VMEM_SPEC,
         scratch_shapes=[
+            *[vm(args[i].shape, args[i].dtype) for i in (0, 1, 6, 7, 9, 10, 11, 12, 13, 14)],
             vm((depth, width), BF16),
             vm((n * slot, depth), BF16),
             vm((8, 3 * LANES), F32),
             vm((n, LANES), F32),
             vm((n, 2, depth // 2, width), BF16),
             vm((width, 4 * LANES), BF16),
+            vm((width, LANES), BF16),
             vm((LANES, width), BF16),
             vm((wo.shape[0], q * LANES), BF16),
             vm((seq + 16, 3 * LANES), F32),
             vm((seq, LANES), BF16),
-            vm((seq, LANES), F32),
+            vm((8, seq), F32),
+            vm((8, seq), F32),
             vm((seq, LANES), BF16),
             vm((seq, LANES), BF16),
             vm((seq, LANES), BF16),
@@ -771,20 +823,21 @@
             vm((q * BLOCK, n * LANES), BF16),
             vm((q, BLOCK, q * LANES), BF16),
             vm((2, q, BLOCK, q * LANES), BF16),
-            dma((q + 1,)), dma((q,)), dma((q, q)), dma((q, q)), dma((q, q)), dma((q, q)),
-            dma((q, 2)), dma((q, 2)), dma((q, q)), dma((q, q)),
-            dma((n, 2)), dma((n, 2)), dma((n,)), dma((n,)), dma((q + 1,)), dma((q,)),
-            dma((q,)), dma((q,)), dma((q, q)), dma((q, q)), dma((q,)), dma((q,)),
-            dma((q,)), dma((q,)), dma((10,)),
+            dma((q + 1,)), dma((q,)), dma((1,)), dma((q, 3)), dma((1,)), dma((q,)),
+            dma((1,)), dma((q,)), dma((1,)), dma((q, 2)), dma((1,)),
+            dma((2,)), dma((2,)), dma((1,)), dma((1,)), dma((q + 1,)), dma((q,)),
+            dma((1,)), dma((q,)), dma((1,)), dma((q, 2)), dma((1,)), dma((1,)), dma((q,)),
+            dma((1,)), dma((1,)), dma((10,)), dma((10,)),
         ],
         compiler_params=pltpu.CompilerParams(
-            collective_id=0, has_side_effects=True, vmem_limit_bytes=VMEM_LIMIT << 20
+            collective_id=0, has_side_effects=True, vmem_limit_bytes=VMEM_LIMIT << 10
         ),
         name="whole",
     )(*args)
 
 
-VMEM_LIMIT = 56
+VMEM_LIMIT = 57344
+HBM_SPEC = pl.BlockSpec(memory_space=pltpu.HBM)
 
 
 def headwise(

time: 122 us -> 114 us (0.934)
  Pallas kernels: 120 us -> 112 us
    pallas_call x1, Pallas kernels: 120 us -> 112 us  [whole(): pl.pallas_call(functools.partial(whole_kernel, n, q), out_shape=jax.Shape...]
where the time goes in v2:
time: 114 us
  Pallas kernels  112 us (98%)
  local copies, waits for them, and re-layouts  1.88 us (2%)
    pallas_call x1, Pallas kernels, whole(): pl.pallas_call(functools.partial(whole_kernel, n, q), out_shape=jax.Shape...  112 us

profile of v2, /device:TPU:0, one launch (start us, length us, event | category | flops | bytes accessed | tf_op | source)
XLA Modules:
  0.0 113.9 jit_solution(4517752815261246259)
XLA Ops:
  0.0 112.0 %whole.1 = bf16[128,2048]{1,0:T(8,128)(2,1)} custom-call(bf16[128,2048]{1,0:T(8,128)(2,1)} %tin_h.1, bf16[2048]{0:T(1024)(128)(2,1)} %ing_h.1, bf16[128,2048]{1,0:T(8,128)(2,1)} %wv.1, bf16[128,2048]{1,0:T(8,128)(2,1)} %wg.1, bf16[128,512]{1,0:T(8,128)(2,1)} %wk.1, bf16[128,512]{1,0:T(8,128)(2,1)} %wr.1, bf16[32,128]{1,0:T(8,128)(2,1)} %bitcast.2, ...), custom_call_target="tpu_custom_call" | custom-call | tf_op jit(solution)/shard_map/whole/pallas_call | solution.py:793
  112.0 1.9 %copy.17 = bf16[128,2048]{1,0:T(8,128)(2,1)} copy(bf16[128,2048]{1,0:T(8,128)(2,1)} %whole.1) | data formatting | bytes 1048576

commit v3 on v2

--- a/solution.py
+++ b/solution.py
@@ -235,10 +235,10 @@
 def whole_kernel(
     n, q, tin_h, ing_h, wv, wg, wk, wr, wsf_h, wsb_h, wo, cv_h, ck_h, cr_h, bias_h, rate_h, ngain_h, out,
     tin, ing, wsf, wsb, cv, ck, cr, bias, rate, ngain,
-    nrm, ws, taps, gains, tok, wts, wgt, wst, wout, raw, gate, pre, sums, vals, keys, reads, cums, yy, injf, injb, carf, carb,
-    nh, full, part, both,
+    nrm, ws, taps, gains, tok, wts, wgt, wst, wout, raw, gate, pre, sums, vals, keys, reads, cums, yy, injf, injb, entered,
+    nh, full, part, other, summed_up, both,
     tzs, tzr, tps, tpr, tss, tsr, kzs, kzr, kps, kpr, kdr, vs, vr, ss, sr, os, orr,
-    as_, ar, bs, br, bdr, es, er, fs, fr, ls, ins,
+    as_, ar, bs, br, bdr, xs, xr, es, er, fs, fr, ls, ins,
 ):
     s, t = lax.axis_index("sp"), lax.axis_index("tp")
     z, p = s // q, s % q
@@ -458,12 +458,21 @@
             plane[e, way] = push(ref, ref, tps.at[0], tpr.at[e, i], side[way])
         swap(e, 0)
 
+    def arrive_last(forwards):
+        zs = sources[q - 1]
+        ok = onward(zs)[1]
+
+        @pl.when(ok if forwards else jnp.logical_not(ok))
+        def _():
+            arrive(q - 1)
+            spread_plane(q - 1)
+
     quarter = half // 2
 
     def relay(e):
         with jax.named_scope("relay"):
             for i, (near_by, other) in enumerate(turns):
-                plane[e, near_by].wait_recv()
+                landed(tok.at[0, 0], tpr.at[e, i])
                 ref = tok.at[sources[e] * q + (px, py)[i], t, pl.ds(i * quarter, quarter)]
                 plane[e, other + "d"] = push(ref, ref, tps.at[0], tpr.at[e, 2], side[other])
                 swap(e, 1 + i)
@@ -559,11 +568,14 @@
             scaled = (val32 * w).astype(BF16)
             dst[i] = jnp.dot(key_t, scaled, preferred_element_type=F32)
 
+    def meet(e):
+        with jax.named_scope("meet"):
+            landed(tok.at[0, 0], tpr.at[e, 2])
+            swap(e, 3)
+
     def use(e):
         zs = sources[e]
         with jax.named_scope("usewait"):
-            landed(tok.at[0, 0], tpr.at[e, 2])
-            swap(e, 3)
             landed(tok.at[pl.ds(0, q if e else q - 1), 0], tsr.at[e])
         with jax.named_scope("project"):
             project(zs)
@@ -630,6 +642,9 @@
     spread_plane(2)
     relay(1)
     send_gates()
+    meet(0)
+    arrive_last(True)
+    chain(wo, wout_of(z), os, orr)
     with jax.named_scope("weights"):
         for copy in locals_:
             copy.wait()
@@ -641,95 +656,95 @@
             chunk = slice(k * LANES, (k + 1) * LANES)
             wts[chunk, 3 * LANES :] = wst[:, chunk].astype(F32).T.astype(BF16)
     use(0)
-    arrive(3)
-    spread_plane(3)
-    chain(wo, wout_of(z), os, orr)
+    meet(1)
     relay(2)
+    arrive_last(False)
     use(1)
+    meet(2)
     relay(3)
     use(2)
+    meet(3)
+    with jax.named_scope("wout1"):
+        wout_onward(1)
+        wout_onward(2)
     with jax.named_scope("gates"):
         landed(wgt.at[pl.ds(0, (n - 1) * depth)], vr.at[1])
     for e in range(q - 1):
         open_gate(sources[e])
-    with jax.named_scope("wout1"):
-        wout_onward(1)
-        wout_onward(2)
     use(3)
 
-    def carry(i, state, d, inj, kept):
-        r0 = pl.multiple_of(i * BLOCK, BLOCK)
-        here = pl.ds(r0, BLOCK)
-        grown = jnp.where(left, cums[here, 16 + 2 * d : 17 + 2 * d], cums[here, 17 + 2 * d : 18 + 2 * d])
-        high = state.astype(BF16)
-        rest = (state - high.astype(F32)).astype(BF16)
-        read = reads[here, :]
-        add = jnp.dot(read, high, preferred_element_type=F32) + jnp.dot(
-            read, rest, preferred_element_type=F32
-        )
-        kept[here, :] = add * grown
-        end = grown[BLOCK - 1 : BLOCK, :] if d == 0 else grown[0:1, :]
-        return state * end + inj[i]
-
-    def advance(i, states):
-        return (
-            carry(i, states[0], 0, injf, carf),
-            carry(blocks - 1 - i, states[1], 1, injb, carb),
-        )
+    def climb(i, states):
+        after = []
+        for d, inj in ((0, injf), (1, injb)):
+            j = i if d == 0 else blocks - 1 - i
+            edge_row = cums[pl.ds(pl.multiple_of(j * BLOCK + (1 - d) * (BLOCK - 8), 8), 8), :]
+            edge_row = edge_row[7:8] if d == 0 else edge_row[0:1]
+            end = jnp.where(left[0:1], edge_row[:, 16 + 2 * d : 17 + 2 * d], edge_row[:, 17 + 2 * d : 18 + 2 * d])
+            high = states[d].astype(BF16)
+            entered[j, :, 2 * d * LANES : (2 * d + 1) * LANES] = high
+            entered[j, :, (2 * d + 1) * LANES : (2 * d + 2) * LANES] = (states[d] - high.astype(F32)).astype(BF16)
+            after.append(states[d] * end + inj[j])
+        return tuple(after)
 
     with jax.named_scope("carry"):
         zero = jnp.zeros((STATE, LANES), F32)
-        lax.fori_loop(0, blocks, advance, (zero, zero), unroll=4)
+        lax.fori_loop(0, blocks, climb, (zero, zero), unroll=4)
 
     gain = gains[pl.ds(s, 1), :]
 
     def finish(i):
         r0 = pl.multiple_of(i * BLOCK, BLOCK)
         here = pl.ds(r0, BLOCK)
-        g = (yy[here, :] + carf[here, :] + carb[here, :]) * silu(gate[here, :].astype(F32))
+        got = jnp.dot(reads[here, :], entered[i], preferred_element_type=F32)
+        y = yy[here, :]
+        for d in range(2):
+            grown = jnp.where(left, cums[here, 16 + 2 * d : 17 + 2 * d], cums[here, 17 + 2 * d : 18 + 2 * d])
+            y = y + (
+                got[:, 2 * d * LANES : (2 * d + 1) * LANES] + got[:, (2 * d + 1) * LANES : (2 * d + 2) * LANES]
+            ) * grown
+        g = y * silu(gate[here, :].astype(F32))
         sq = g * g
         m0 = jnp.sum(jnp.where(left, sq, 0.0), -1, keepdims=True) / HEAD_DIM
         m1 = jnp.sum(jnp.where(left, 0.0, sq), -1, keepdims=True) / HEAD_DIM
         scale = jnp.where(left, lax.rsqrt(m0 + EPSILON), lax.rsqrt(m1 + EPSILON))
         nh[here, :] = (g * scale * gain).astype(BF16)
 
-    away = []
-    for dz in range(1, q + 1):
-        to = lax.rem(z + dz, q)
-
+    def finish_plane(zs):
         with jax.named_scope("finish"):
 
             @pl.loop(0, q, unroll=4)
             def _(i):
-                finish(to * q + i)
-
-        if dz < q:
-            away.append(
-                push(nh.at[span(to, q * BLOCK)], full.at[:, mine], as_.at[0], ar.at[dz], (at(dz, 0), t))
-            )
+                finish(zs * q + i)
+
     near = {}
-    keep = local(nh.at[span(z, q * BLOCK)], full.at[:, mine], 8)
-    for i, to in enumerate("xy"):
-        near[0, to] = push(
-            nh.at[span(z, q * BLOCK)], full.at[:, mine], bs.at[0], br.at[0, i], side[to]
-        )
-    rest_rows = q * BLOCK // 2
-
-    def near_relay(dz):
+
+    def spread_near(e):
+        ref = full.at[:, span(sources[e] * q + p, LANES)] if e else nh.at[span(z, q * BLOCK)]
+        dst = full.at[:, span(sources[e] * q + p, LANES)]
+        for i, to in enumerate("xy"):
+            near[e, to] = push(ref, dst, bs.at[0], br.at[e, i], side[to])
+
+    def near_relay(e):
         with jax.named_scope("nearwait"):
             for i, (near_by, other) in enumerate(turns):
-                near[dz, near_by].wait_recv()
-                got = full.at[pl.ds(i * rest_rows, rest_rows), span(chip(dz, (px, py)[i]), LANES)]
-                near[dz, other + "d"] = push(got, got, bs.at[0], bdr.at[0], side[other])
-
-    for dz in range(1, q):
+                near[e, near_by].wait_recv()
+                got = full.at[pl.ds(i * rest_rows, rest_rows), span(sources[e] * q + (px, py)[i], LANES)]
+                push(got, got, bs.at[0], bdr.at[0], side[other])
+
+    rest_rows = q * BLOCK // 2
+    for e in range(1, q):
+        zs = sources[e]
+        finish_plane(zs)
+        push(nh.at[span(zs, q * BLOCK)], full.at[:, mine], as_.at[0], ar.at[z], (zs * q + p, t))
+    finish_plane(z)
+    keep = local(nh.at[span(z, q * BLOCK)], full.at[:, mine], 8)
+    spread_near(0)
+    for e in range(1, q):
         with jax.named_scope("awaywait"):
-            away[dz - 1].wait_recv()
-        got = full.at[:, span(at(q - dz, 0), LANES)]
-        for i, to in enumerate("xy"):
-            near[dz, to] = push(got, got, bs.at[0], br.at[dz, i], side[to])
-        near_relay(dz - 1)
-        if dz == 2:
+            landed(nh.at[pl.ds(0, q * BLOCK)], ar.at[sources[e]])
+        spread_near(e)
+        near_relay(e - 1)
+        if e == 2:
             with jax.named_scope("wout2"):
                 wout_onward(3)
     near_relay(q - 1)
@@ -740,33 +755,53 @@
         keep.wait()
         landed(full.at[pl.ds(0, BLOCK)], bdr.at[0])
     legs = []
-
-    def leg(dp):
-        to = lax.rem(p + dp, q)
-        legs.append(push(part.at[to], both.at[t, p], es.at[0], er.at[dp], (at(0, dp), t)))
+    part_rows = BLOCK // 2
+    kept, given = span(t, part_rows), span(1 - t, part_rows)
+
+    def toward(dp):
+        return lax.rem(p + dp, q)
+
+    def multiply(dp):
+        to = toward(dp)
+        part[to] = jnp.dot(full[span(to, BLOCK), :], wout[...], preferred_element_type=F32).astype(BF16)
+
+    def give(dp):
+        to = toward(dp)
+        push(part.at[to, given], other.at[to], xs.at[0], xr.at[dp - 1], sibling)
+
+    def add_up(dp):
+        to = toward(dp)
+        landed(other.at[to], xr.at[dp - 1])
+        total = (part[to, kept, :].astype(F32) + other[to].astype(F32)).astype(BF16)
+        if dp < q:
+            summed_up[to] = total
+            legs.append(push(summed_up.at[to], both.at[t, p], es.at[0], er.at[dp], (at(0, dp), t)))
+        else:
+            both[t, p] = total
+            push(both.at[t, p], both.at[t, p], fs.at[0], fr.at[0], sibling)
 
     with jax.named_scope("outdot"):
+        multiply(1)
+        for dp in range(2, q + 1):
+            multiply(dp)
+            give(dp - 1)
+        give(q)
         for dp in range(1, q + 1):
-            to = lax.rem(p + dp, q)
-            part[to] = jnp.dot(full[span(to, BLOCK), :], wout[...], preferred_element_type=F32).astype(BF16)
-            if dp >= 2:
-                leg(dp - 1)
-    across = [push(part.at[p], both.at[t, p], fs.at[0], fr.at[0], sibling)]
-    keep = local(part.at[p], both.at[t, p], 9)
+            add_up(dp)
     with jax.named_scope("legswait"):
         for dp in range(1, q):
             legs[dp - 1].wait_recv()
             got = both.at[t, lax.rem(p + q - dp, q)]
-            across.append(push(got, got, fs.at[0], fr.at[0], sibling))
+            push(got, got, fs.at[0], fr.at[0], sibling)
     with jax.named_scope("acrosswait"):
-        keep.wait()
-        landed(part, fr.at[0])
+        landed(both.at[0], fr.at[0])
     with jax.named_scope("sum"):
-        for a in range(q):
-            for b in range(q):
-                here = slice(a * LANES, (a + 1) * LANES)
-                total = both[0, b, :, here].astype(F32) + both[1, b, :, here].astype(F32)
-                out[:, (a * q + b) * LANES : (a * q + b + 1) * LANES] = total.astype(BF16)
+        for h in range(2):
+            for a in range(q):
+                for b in range(q):
+                    out[h * part_rows : (h + 1) * part_rows, (a * q + b) * LANES : (a * q + b + 1) * LANES] = both[
+                        h, b, :, a * LANES : (a + 1) * LANES
+                    ]
     with jax.named_scope("sends"):
         settle_chain(unit, tzs, tzr, tok_of)
         settle_chain(wo, os, orr, wout_of)
@@ -779,8 +814,9 @@
         left_here(ws.at[pl.ds(0, (n - 1) * slot)], ss.at[0])
         left_here(nh.at[pl.ds(0, (q - 1) * q * BLOCK)], as_.at[0])
         left_here(full.at[pl.ds(0, 3 * BLOCK)], bs.at[0])
-        left_here(part.at[pl.ds(0, q - 1)], es.at[0])
-        left_here(part, fs.at[0])
+        left_here(other, xs.at[0])
+        left_here(summed_up.at[pl.ds(0, q - 1)], es.at[0])
+        left_here(both.at[0], fs.at[0])
 
 
 def whole(n, q, *args):
@@ -817,16 +853,17 @@
             vm((seq, LANES), F32),
             vm((seq // BLOCK, STATE, LANES), F32),
             vm((seq // BLOCK, STATE, LANES), F32),
-            vm((seq, LANES), F32),
-            vm((seq, LANES), F32),
+            vm((seq // BLOCK, STATE, 4 * LANES), BF16),
             vm((seq, LANES), BF16),
             vm((q * BLOCK, n * LANES), BF16),
             vm((q, BLOCK, q * LANES), BF16),
-            vm((2, q, BLOCK, q * LANES), BF16),
+            vm((q, BLOCK // 2, q * LANES), BF16),
+            vm((q, BLOCK // 2, q * LANES), BF16),
+            vm((2, q, BLOCK // 2, q * LANES), BF16),
             dma((q + 1,)), dma((q,)), dma((1,)), dma((q, 3)), dma((1,)), dma((q,)),
             dma((1,)), dma((q,)), dma((1,)), dma((q, 2)), dma((1,)),
             dma((2,)), dma((2,)), dma((1,)), dma((1,)), dma((q + 1,)), dma((q,)),
-            dma((1,)), dma((q,)), dma((1,)), dma((q, 2)), dma((1,)), dma((1,)), dma((q,)),
+            dma((1,)), dma((q,)), dma((1,)), dma((q, 2)), dma((1,)), dma((1,)), dma((q,)), dma((1,)), dma((q,)),
             dma((1,)), dma((1,)), dma((10,)), dma((10,)),
         ],
         compiler_params=pltpu.CompilerParams(

time: 114 us -> 112 us (0.982)
  Pallas kernels: 112 us -> 110 us
    pallas_call x1, Pallas kernels: 112 us -> 110 us  [whole(): pl.pallas_call(functools.partial(whole_kernel, n, q), out_shape=jax.Shape...]
where the time goes in v3:
time: 112 us
  Pallas kernels  110 us (98%)
  local copies, waits for them, and re-layouts  1.88 us (2%)
    pallas_call x1, Pallas kernels, whole(): pl.pallas_call(functools.partial(whole_kernel, n, q), out_shape=jax.Shape...  110 us

profile of v3, /device:TPU:0, one launch (start us, length us, event | category | flops | bytes accessed | tf_op | source)
XLA Modules:
  0.0 111.9 jit_solution(8919901670797315892)
XLA Ops:
  0.0 110.0 %whole.1 = bf16[128,2048]{1,0:T(8,128)(2,1)} custom-call(bf16[128,2048]{1,0:T(8,128)(2,1)} %tin_h.1, bf16[2048]{0:T(1024)(128)(2,1)} %ing_h.1, bf16[128,2048]{1,0:T(8,128)(2,1)} %wv.1, bf16[128,2048]{1,0:T(8,128)(2,1)} %wg.1, bf16[128,512]{1,0:T(8,128)(2,1)} %wk.1, bf16[128,512]{1,0:T(8,128)(2,1)} %wr.1, bf16[32,128]{1,0:T(8,128)(2,1)} %bitcast.2, ...), custom_call_target="tpu_custom_call" | custom-call | tf_op jit(solution)/shard_map/whole/pallas_call | solution.py:829
  110.0 1.9 %copy.17 = bf16[128,2048]{1,0:T(8,128)(2,1)} copy(bf16[128,2048]{1,0:T(8,128)(2,1)} %whole.1) | data formatting | bytes 1048576

commit v4 on v3

--- a/solution.py
+++ b/solution.py
@@ -536,6 +536,11 @@
             here = pl.ds(pl.multiple_of(zs * q * BLOCK, q * BLOCK), q * BLOCK)
             gate[here, :] = jnp.dot(x, wgt[...], preferred_element_type=F32).astype(BF16)
 
+    def open_block(i):
+        here = pl.ds(pl.multiple_of(i * BLOCK, BLOCK), BLOCK)
+        x = tok[i].reshape(BLOCK, tok.shape[3])
+        gate[here, :] = jnp.dot(x, wgt[...], preferred_element_type=F32).astype(BF16)
+
     def convolve(i):
         r0 = pl.multiple_of(i * BLOCK, BLOCK)
         for b, dst in enumerate((vals, keys, reads)):
@@ -590,8 +595,6 @@
         def which(i):
             return start + i if e < q - 1 else jnp.where(i < q, start + i, edge)
 
-        if e == q - 1:
-            open_gate(zs)
         with jax.named_scope("conv"):
 
             @pl.loop(0, count, unroll=count)
@@ -602,6 +605,8 @@
 
             @pl.loop(0, count, unroll=count)
             def _(i):
+                if e == q - 1:
+                    open_block(zs * q + jnp.minimum(i, q - 1))
                 within(which(i))
 
         if e < q - 1:
@@ -662,11 +667,11 @@
     use(1)
     meet(2)
     relay(3)
-    use(2)
-    meet(3)
     with jax.named_scope("wout1"):
         wout_onward(1)
         wout_onward(2)
+    use(2)
+    meet(3)
     with jax.named_scope("gates"):
         landed(wgt.at[pl.ds(0, (n - 1) * depth)], vr.at[1])
     for e in range(q - 1):

time: 112 us -> 111 us (level)
    pallas_call x1, Pallas kernels: 110 us -> 109 us  [whole(): pl.pallas_call(functools.partial(whole_kernel, n, q), out_shape=jax.Shape...]
where the time goes in v4:
time: 111 us
  Pallas kernels  109 us (98%)
  local copies, waits for them, and re-layouts  1.88 us (2%)
    pallas_call x1, Pallas kernels, whole(): pl.pallas_call(functools.partial(whole_kernel, n, q), out_shape=jax.Shape...  109 us

profile of v4, /device:TPU:0, one launch (start us, length us, event | category | flops | bytes accessed | tf_op | source)
XLA Modules:
  0.0 110.6 jit_solution(2080595052990218561)
XLA Ops:
  0.0 108.7 %whole.1 = bf16[128,2048]{1,0:T(8,128)(2,1)} custom-call(bf16[128,2048]{1,0:T(8,128)(2,1)} %tin_h.1, bf16[2048]{0:T(1024)(128)(2,1)} %ing_h.1, bf16[128,2048]{1,0:T(8,128)(2,1)} %wv.1, bf16[128,2048]{1,0:T(8,128)(2,1)} %wg.1, bf16[128,512]{1,0:T(8,128)(2,1)} %wk.1, bf16[128,512]{1,0:T(8,128)(2,1)} %wr.1, bf16[32,128]{1,0:T(8,128)(2,1)} %bitcast.2, ...), custom_call_target="tpu_custom_call" | custom-call | tf_op jit(solution)/shard_map/whole/pallas_call | solution.py:834
  108.7 1.9 %copy.17 = bf16[128,2048]{1,0:T(8,128)(2,1)} copy(bf16[128,2048]{1,0:T(8,128)(2,1)} %whole.1) | data formatting | bytes 1048576

commit v5 on v4

--- a/solution.py
+++ b/solution.py
@@ -666,10 +666,10 @@
     arrive_last(False)
     use(1)
     meet(2)
-    relay(3)
     with jax.named_scope("wout1"):
         wout_onward(1)
         wout_onward(2)
+    relay(3)
     use(2)
     meet(3)
     with jax.named_scope("gates"):

time: 111 us -> 111 us (level)
  no operation moved by 1% of the time
where the time goes in v5:
time: 111 us; the launch traced here: 110 us
  Pallas kernels  108 us (97%)
  local copies, waits for them, and re-layouts  1.88 us (2%)
    pallas_call x1, Pallas kernels, whole(): pl.pallas_call(functools.partial(whole_kernel, n, q), out_shape=jax.Shape...  108 us

profile of v5, /device:TPU:0, one launch (start us, length us, event | category | flops | bytes accessed | tf_op | source)
XLA Modules:
  0.0 110.4 jit_solution(4509633180681246306)
XLA Ops:
  0.0 108.5 %whole.1 = bf16[128,2048]{1,0:T(8,128)(2,1)} custom-call(bf16[128,2048]{1,0:T(8,128)(2,1)} %tin_h.1, bf16[2048]{0:T(1024)(128)(2,1)} %ing_h.1, bf16[128,2048]{1,0:T(8,128)(2,1)} %wv.1, bf16[128,2048]{1,0:T(8,128)(2,1)} %wg.1, bf16[128,512]{1,0:T(8,128)(2,1)} %wk.1, bf16[128,512]{1,0:T(8,128)(2,1)} %wr.1, bf16[32,128]{1,0:T(8,128)(2,1)} %bitcast.2, ...), custom_call_target="tpu_custom_call" | custom-call | tf_op jit(solution)/shard_map/whole/pallas_call | solution.py:834
  108.5 1.9 %copy.17 = bf16[128,2048]{1,0:T(8,128)(2,1)} copy(bf16[128,2048]{1,0:T(8,128)(2,1)} %whole.1) | data formatting | bytes 1048576
